TPU v7x, 512 devices: a 8x2x16 block of a 8x8x16 slice. The times are simulated.
512 devices in a mesh: grp: 2 (over y), sp: 32 (over z, core), tp: 8 (over x).
Axes of the slice: x: 8, y: 2, z: 16, core: 2. Of those that a mesh axis runs over, the one named last changes fastest.
The devices are a block of a 8x8x16 slice.
Arguments:
- tokens: bfloat16 [32768, 2048], P(('grp', 'sp'), 'tp'), parts along dimension 0, may hold values from -140 to 140, as said below
- mix_gain: bfloat16 [2, 2048], replicated, may hold values from 0.099609375 to 1.8984375
- gate_weight: bfloat16 [2, 2048, 2048], P(None, 'sp', 'tp'), may hold values from -0.125 to 0.125
- mix_weight: bfloat16 [2, 2048, 2048], P(None, 'sp', 'tp'), may hold values from -0.125 to 0.125
- value_weight: bfloat16 [2, 2048, 2048], P(None, 'sp', 'tp'), may hold values from -0.125 to 0.125
- out_weight: bfloat16 [2, 2048, 2048], P(None, 'sp', 'tp'), may hold values from -0.125 to 0.125
- conv_taps: bfloat16 [2, 3, 2048], P(None, None, 'tp'), may hold values from -3.5 to 3.5
Outputs:
- result_stream: bfloat16 [32768, 2048], P(('grp', 'sp'), 'tp'), parts along dimension 0
There are 2 independent parts, one for each index of `grp`. A program takes and returns all parts, laid end to end along the dimension named above; an argument that names none is the same for every part. Nothing has to cross between parts.
Inputs may be any that keep to these rules, and one draw needn't show every extreme that they name: `tokens`: activations with feature scales of several sizes.
All inputs are finite; a program needn't handle non-finite values.
Results may differ from a plain program's by a relative error of at most 0.015.
Values may be sent and summed in bfloat16 or wider, within the bound.
No kernel may reach another device: no remote copies, remote signals or barrier semaphores. Data moves between devices by JAX's collectives and lax.ppermute only.
A program may use at most 64 MiB of HBM per device.

v0:
```python
import jax
import jax.numpy as jnp
from jax import lax
from jax.sharding import PartitionSpec as P

EPS = 1e-06


def passed_along(x, axis, by):
    devices = lax.axis_size(axis)
    pairs = [(i, i + by) for i in range(devices) if 0 <= i + by < devices]
    return lax.ppermute(x, axis, pairs)


def in_one_piece(arrays, axis, dim, along):
    ends, at = ([], 0)
    for a in arrays[:-1]:
        at += a.shape[along]
        ends.append(at)
    both = jnp.concatenate(arrays, axis=along)
    return tuple(jnp.split(lax.all_gather(both, axis, axis=dim, tiled=True), ends, axis=along))


def in_order(pieces, dim):
    dims = list(pieces.shape[1:])
    dims[dim] *= pieces.shape[0]
    return jnp.moveaxis(pieces, 0, dim).reshape(dims)


def copy_for_each(x, axis):
    copies = jnp.broadcast_to(x, (lax.axis_size(axis), *x.shape))
    return lax.all_to_all(copies, axis, split_axis=0, concat_axis=0, tiled=True)


def collect(x, axis, dim):
    return in_order(copy_for_each(x, axis), dim)


def normed_rows(rows, gain):
    wide_rows = rows.astype(jnp.float32)
    factor = lax.rsqrt(jnp.mean(wide_rows * wide_rows, axis=1, keepdims=True) + EPS)
    return (wide_rows * factor * gain.astype(jnp.float32)).astype(jnp.bfloat16)


def convolve(carried, before, tap_rows):
    padded = jnp.concatenate([before, carried], axis=0)
    row_count = carried.shape[0]
    result = jnp.zeros_like(carried)
    for tap_index in range(tap_rows.shape[0]):
        result = (
            result
            + tap_rows[tap_index].astype(jnp.float32) * padded[tap_index : tap_index + row_count]
        )
    return result


def shards(tokens, mix_gain, gate_weight, mix_weight, value_weight, out_weight, conv_taps):
    layer_count = gate_weight.shape[0]
    conv_reach = conv_taps.shape[1] - 1
    fringe_depth = conv_reach * layer_count
    before_rows = passed_along(tokens[tokens.shape[0] - fringe_depth :], "sp", 1)
    stream = jnp.concatenate([before_rows, tokens], axis=0)
    gathered = in_one_piece((gate_weight, mix_weight, value_weight, out_weight), "sp", 1, 0)
    channels = gate_weight.shape[2]
    for layer_index in range(layer_count):
        whole = collect(stream, "tp", 1)
        normed = normed_rows(whole, mix_gain[layer_index])
        gate = jnp.dot(normed, gathered[0][layer_index], preferred_element_type=jnp.float32)
        inner = jnp.dot(normed, gathered[1][layer_index], preferred_element_type=jnp.float32)
        values = jnp.dot(normed, gathered[2][layer_index], preferred_element_type=jnp.float32)
        gate = gate.astype(jnp.bfloat16)
        inner = inner.astype(jnp.bfloat16)
        values = values.astype(jnp.bfloat16)
        carried = inner.astype(jnp.float32) * values.astype(jnp.float32)
        before = jnp.zeros((conv_reach, channels), jnp.float32)
        conv = convolve(carried, before, conv_taps[layer_index])
        mixed = (gate.astype(jnp.float32) * conv).astype(jnp.bfloat16)
        mixed_all = lax.all_gather(mixed, "tp", axis=1, tiled=True)
        product = jnp.dot(mixed_all, gathered[3][layer_index], preferred_element_type=jnp.float32)
        stream = (stream.astype(jnp.float32) + product).astype(jnp.bfloat16)
    return stream[fringe_depth:]


def solution(mesh):
    return jax.shard_map(
        shards,
        mesh=mesh,
        in_specs=(
            P(("grp", "sp"), "tp"),
            P(),
            P(None, "sp", "tp"),
            P(None, "sp", "tp"),
            P(None, "sp", "tp"),
            P(None, "sp", "tp"),
            P(None, None, "tp"),
        ),
        out_specs=P(("grp", "sp"), "tp"),
        check_vma=False,
    )
```

profile of v0, /device:TPU:80, one launch (start us, length us, event | category | flops | bytes accessed | tf_op | source)
XLA Modules:
  0.0 305.4 jit_solution(15098368979078359198)
XLA Ops:
  6.5 0.0 all-gather.4.cloned.1.call-start
  6.6 1.7 pad_maximum_fusion.1
  8.2 0.1 all-gather.4.cloned.1.call-update
  8.3 0.7 slice.88
  9.0 1.8 collective-permute-start
  10.8 0.8 collective-permute-done
  11.6 1.0 pad_maximum_fusion
  12.6 1.5 broadcast_in_dim.4
  14.1 0.0 copy-start.1
  14.1 0.0 copy-start.2
  14.1 7.4 %all-to-all-start = ((bf16[8,516,256]{2,1,0:T(8,128)(2,1)}), bf16[8,516,256]{2,1,0:T(8,128)(2,1)S(1)}, u32[]{:S(2)}, u32[]{:S(2)}) async-start(bf16[8,516,256]{2,1,0:T(8,128)(2,1)} %broadcast_in_dim.4), calls=%async_computation | async-start | bytes 4259840 | tf_op jit(solution)/shard_map/all_to_all | solution.py:32
  21.6 0.1 all-gather.6.cloned.1.call-start
  21.7 0.0 copy-done.1
  21.7 0.0 copy-done.2
  21.8 53.0 %all-to-all-done = bf16[8,516,256]{2,1,0:T(8,128)(2,1)S(1)} async-done(((bf16[8,516,256]{2,1,0:T(8,128)(2,1)}), bf16[8,516,256]{2,1,0:T(8,128)(2,1)S(1)}, u32[]{:S(2)}, u32[]{:S(2)}) %all-to-all-start) | async-done | bytes 2113568 | tf_op jit(solution)/shard_map/all_to_all | solution.py:32
  74.8 0.5 fusion
  75.3 0.6 fusion.7
  75.9 0.4 copy.8
  76.3 0.1 pad.8
  76.5 0.7 copy.10
  77.2 45.6 %all-gather.4.cloned.1.call-done = bf16[8,2048,256]{2,1,0:T(8,128)(2,1)} async-done(((bf16[8,64,256]{2,1,0:T(8,128)(2,1)}), bf16[8,2048,256]{2,1,0:T(8,128)(2,1)}) %all-gather.4.cloned.1.call-update) | async-done | bytes 8388624 | tf_op jit(solution)/shard_map/all_gather | solution.py:21
  122.8 2.0 fusion.13
  124.8 2.0 fusion.12
  126.8 0.0 copy-start
  126.8 2.7 fusion.10
  129.5 0.1 all-gather.6.cloned.1.call-update
  129.6 50.5 %all-gather.6.cloned.1.call-done = bf16[516,2048]{1,0:T(8,128)(2,1)} async-done(((bf16[516,256]{1,0:T(8,128)(2,1)}), bf16[516,2048]{1,0:T(8,128)(2,1)}) %all-gather.6.cloned.1.call-update) | async-done | bytes 2113552 | tf_op jit(solution)/shard_map/all_gather | solution.py:78
  180.0 0.0 copy-done
  180.1 2.6 add_convert_fusion
  182.7 1.5 broadcast_in_dim.5
  184.2 4.4 %all-to-all-start.1 = ((bf16[8,516,256]{2,1,0:T(8,128)(2,1)}), bf16[8,516,256]{2,1,0:T(8,128)(2,1)S(1)}, u32[]{:S(2)}, u32[]{:S(2)}) async-start(bf16[8,516,256]{2,1,0:T(8,128)(2,1)} %broadcast_in_dim.5), calls=%async_computation.1 | async-start | bytes 4259840 | tf_op jit(solution)/shard_map/all_to_all | solution.py:32
  188.5 0.2 all-gather.8.cloned.1.call-start
  188.8 46.6 %all-to-all-done.1 = bf16[8,516,256]{2,1,0:T(8,128)(2,1)S(1)} async-done(((bf16[8,516,256]{2,1,0:T(8,128)(2,1)}), bf16[8,516,256]{2,1,0:T(8,128)(2,1)S(1)}, u32[]{:S(2)}, u32[]{:S(2)}) %all-to-all-start.1) | async-done | bytes 2113568 | tf_op jit(solution)/shard_map/all_to_all | solution.py:32
  235.4 0.5 fusion.3
  235.9 0.6 fusion.6
  236.5 0.4 copy.9
  236.9 0.1 pad.9
  237.1 0.7 copy.11
  237.8 2.0 fusion.19
  239.8 2.0 fusion.18
  241.8 2.7 fusion.16
  244.5 0.1 all-gather.8.cloned.1.call-update
  244.6 50.9 %all-gather.8.cloned.1.call-done = bf16[516,2048]{1,0:T(8,128)(2,1)} async-done(((bf16[516,256]{1,0:T(8,128)(2,1)}), bf16[516,2048]{1,0:T(8,128)(2,1)}) %all-gather.8.cloned.1.call-update) | async-done | bytes 2113552 | tf_op jit(solution)/shard_map/all_gather | solution.py:78
  295.4 2.6 fusion.20
  298.0 0.8 fusion.22
  (6 shorter events, 0.1 us)
Async XLA Ops:
  6.5 116.2 %all-gather.4.cloned.1.call-start = ((), (), s32[]{:S(2)}) async-start(), calls=%async_computation.2 | async-start | bytes 8650752 | tf_op jit(solution)/shard_map/all_gather | solution.py:21
  9.0 2.6 collective-permute-start
  14.1 7.5 %copy-start.1 = (bf16[2,2048]{1,0:T(2,128)(2,1)S(1)}, bf16[2,2048]{1,0:T(2,128)(2,1)}, u32[]{:S(2)}) copy-start(bf16[2,2048]{1,0:T(2,128)(2,1)} %param.8) | copy-start | bytes 24580
  14.1 7.6 %copy-start.2 = (bf16[2,3,256]{2,0,1:T(2,128)(2,1)S(1)}, bf16[2,3,256]{2,0,1:T(2,128)(2,1)}, u32[]{:S(2)}) copy-start(bf16[2,3,256]{2,0,1:T(2,128)(2,1)} %param.13) | copy-start | bytes 9220
  14.1 60.7 %all-to-all-start = ((bf16[8,516,256]{2,1,0:T(8,128)(2,1)}), bf16[8,516,256]{2,1,0:T(8,128)(2,1)S(1)}, u32[]{:S(2)}, u32[]{:S(2)}) async-start(bf16[8,516,256]{2,1,0:T(8,128)(2,1)} %broadcast_in_dim.4), calls=%async_computation | async-start | bytes 4259840 | tf_op jit(solution)/shard_map/all_to_all | solution.py:32
  21.6 158.5 %all-gather.6.cloned.1.call-start = ((), (), s32[]{:S(2)}) async-start(), calls=%async_computation.3 | async-start | bytes 2396160 | tf_op jit(solution)/shard_map/all_gather | solution.py:78
  126.8 53.3 %copy-start = (bf16[512,256]{1,0:T(8,128)(2,1)S(1)}, bf16[512,256]{1,0:T(8,128)(2,1)}, u32[]{:S(2)}) copy-start(bf16[512,256]{1,0:T(8,128)(2,1)} %param.7) | copy-start | bytes 786436
  184.2 51.3 %all-to-all-start.1 = ((bf16[8,516,256]{2,1,0:T(8,128)(2,1)}), bf16[8,516,256]{2,1,0:T(8,128)(2,1)S(1)}, u32[]{:S(2)}, u32[]{:S(2)}) async-start(bf16[8,516,256]{2,1,0:T(8,128)(2,1)} %broadcast_in_dim.5), calls=%async_computation.1 | async-start | bytes 4259840 | tf_op jit(solution)/shard_map/all_to_all | solution.py:32
  188.5 106.9 %all-gather.8.cloned.1.call-start = ((), (), s32[]{:S(2)}) async-start(), calls=%async_computation.4 | async-start | bytes 2396160 | tf_op jit(solution)/shard_map/all_gather | solution.py:78
Sparse Core Ops, SparseCore 0:
  9.5 113.2 all-gather.3
  129.7 50.2 all-gather.5
  244.7 50.6 all-gather.7
where the time goes:
time: 307 us; the launch traced here: 305 us
  waiting for transfers between devices  248 us (81%)
  matrix products  18.6 us (6%)
  starting transfers between devices  14 us (5%)
  between operations  13.3 us (4%)
  local copies, waits for them, and re-layouts  6.28 us (2%)
  other arithmetic  5.67 us (2%)
    all_gather x2, waiting for transfers between devices, shards(): mixed_all = lax.all_gather(mixed, 'tp', axis=1, tiled=True)  101 us
    all_to_all x2, waiting for transfers between devices, copy_for_each(): return lax.all_to_all(copies, axis, split_axis=0, concat_axis=0, tiled=True)  99.7 us
    all_gather x1, waiting for transfers between devices, in_one_piece(): lax.all_gather(both, axis, axis=dim, tiled=True)  45.6 us
    all_to_all x2, starting transfers between devices, copy_for_each(): return lax.all_to_all(copies, axis, split_axis=0, concat_axis=0, tiled=True)  11.8 us
  transfers between devices with their start and end apart: 6, of which 6 were waited for; matrix products, arithmetic and copies ran while one was open for 2% of the time, Pallas kernels for 0%

commit v1 on v0

v1 whole, which is shorter than its diff:
```python
import jax
import jax.numpy as jnp
from jax import lax
from jax.sharding import PartitionSpec as P

EPS = 1e-06
TILE_ROWS = 8
F32 = jnp.float32
BF16 = jnp.bfloat16


def passed_along(x, axis, by):
    devices = lax.axis_size(axis)
    pairs = [(i, i + by) for i in range(devices) if 0 <= i + by < devices]
    return lax.ppermute(x, axis, pairs)


def turned(x, axis, by):
    devices = lax.axis_size(axis)
    return lax.ppermute(x, axis, [(i, (i + by) % devices) for i in range(devices)])


def ring(block, axis):
    devices = lax.axis_size(axis)
    arrived = [(0, block)]
    up = down = block
    for step in range(1, (devices - 1) // 2 + 1):
        up, down = turned(up, axis, 1), turned(down, axis, -1)
        arrived += [(-step, up), (step, down)]
    if devices % 2 == 0:
        half = block.shape[0] // 16 * 8
        up, down = turned(up[:half], axis, 1), turned(down[half:], axis, -1)
        arrived.append((devices // 2, jnp.concatenate([up, down], axis=0)))
    return arrived


def rows_of(weight, owner, count):
    return lax.dynamic_slice_in_dim(weight, owner * count, count, axis=0)


def convolve(carried, tap_rows):
    reach = tap_rows.shape[0] - 1
    count = carried.shape[0]
    padded = jnp.concatenate([jnp.zeros((reach, carried.shape[1]), F32), carried], axis=0)
    result = jnp.zeros_like(carried)
    for tap in range(reach + 1):
        result = result + tap_rows[tap].astype(F32) * padded[tap : tap + count]
    return result


def shards(tokens, mix_gain, gate_weight, mix_weight, value_weight, out_weight, conv_taps):
    layers, _, width = gate_weight.shape
    devices = lax.axis_size("tp")
    me = lax.axis_index("tp")
    reach = conv_taps.shape[1] - 1
    fringe = -(-reach * layers // TILE_ROWS) * TILE_ROWS
    before = passed_along(tokens[tokens.shape[0] - fringe :], "sp", 1)
    stream = jnp.concatenate([before, tokens], axis=0)

    mine = jnp.concatenate(
        [w[l] for l in range(layers) for w in (gate_weight, mix_weight, value_weight, out_weight)], axis=0
    ).reshape(layers * 4, -1, width)
    whole = lax.all_gather(mine, "sp", axis=1, tiled=True)

    for l in range(layers):
        gains = mix_gain[l].reshape(devices, 1, width)
        total = [None] * 3
        squares = 0.0
        for offset, block in ring(stream, "tp"):
            owner = lax.rem(me + offset + devices, devices)
            wide = block.astype(F32)
            squares = squares + jnp.sum(wide * wide, axis=1, keepdims=True)
            scaled = (wide * lax.dynamic_index_in_dim(gains, owner, 0, False).astype(F32)).astype(BF16)
            for k in range(3):
                part = jnp.dot(scaled, rows_of(whole[4 * l + k], owner, width), preferred_element_type=F32)
                total[k] = part if total[k] is None else total[k] + part
        factor = lax.rsqrt(squares / (devices * width) + EPS)
        gate, inner, values = ((t * factor).astype(BF16).astype(F32) for t in total)
        mixed = (gate * convolve(inner * values, conv_taps[l])).astype(BF16)
        product = stream.astype(F32)
        for offset, block in ring(mixed, "tp"):
            owner = lax.rem(me + offset + devices, devices)
            product = product + jnp.dot(block, rows_of(whole[4 * l + 3], owner, width), preferred_element_type=F32)
        stream = product.astype(BF16)
    return stream[fringe:]


def solution(mesh):
    return jax.shard_map(
        shards,
        mesh=mesh,
        in_specs=(
            P(("grp", "sp"), "tp"),
            P(),
            P(None, "sp", "tp"),
            P(None, "sp", "tp"),
            P(None, "sp", "tp"),
            P(None, "sp", "tp"),
            P(None, None, "tp"),
        ),
        out_specs=P(("grp", "sp"), "tp"),
        check_vma=False,
    )
```

time: 307 us -> 302 us (0.984)
  waiting for transfers between devices: 248 us -> 124 us
  starting transfers between devices: 14 us -> 117 us
  local copies, waits for them, and re-layouts: 6.28 us -> 14.9 us
  matrix products: 18.6 us -> 24.9 us
    ppermute x0 -> x32, starting transfers between devices: none -> 115 us  [turned(): lax.ppermute(x, axis, [(i, (i + by) % devices) for i in range(devices)])]
    all_to_all x2 -> x0, waiting for transfers between devices: 99.7 us -> none  [copy_for_each(): return lax.all_to_all(copies, axis, split_axis=0, concat_axis=0, tiled=True)]
    all_gather x3 -> x1, waiting for transfers between devices: 147 us -> 60.5 us  [shards(): whole = lax.all_gather(mine, 'sp', axis=1, tiled=True)]
    ppermute x0 -> x32, waiting for transfers between devices: none -> 62.9 us  [turned(): lax.ppermute(x, axis, [(i, (i + by) % devices) for i in range(devices)])]
    all_to_all x2 -> x0, starting transfers between devices: 11.8 us -> none  [copy_for_each(): return lax.all_to_all(copies, axis, split_axis=0, concat_axis=0, tiled=True)]
    slice x1 -> x11, local copies, waits for them, and re-layouts: 0.69 us -> 7.11 us  [the longest x1 5.51 us: shards(): whole[4 * l + 3]]
    dot_general x8 -> x64, matrix products: 18.6 us -> 24.9 us  [the longest x48 13.6 us: shards(): jnp.dot(scaled, rows_of(whole[4 * l + k], owner, width), preferred_elemen...]
    unnamed x10 -> x16, local copies, waits for them, and re-layouts: 1.7 us -> 6.04 us
  transfers between devices with their start and end apart: 6 -> 34, of which waited for: 6 -> 20; matrix products, arithmetic and copies ran while one was open for 2% -> 7% of each run, Pallas kernels for 0% -> 0%
where the time goes in v1:
time: 302 us; the launch traced here: 300 us
  waiting for transfers between devices  124 us (41%)
  starting transfers between devices  117 us (39%)
  matrix products  24.9 us (8%)
  local copies, waits for them, and re-layouts  14.9 us (5%)
  between operations  14.5 us (5%)
  other arithmetic  4.44 us (1%)
    ppermute x32, starting transfers between devices, turned(): lax.ppermute(x, axis, [(i, (i + by) % devices) for i in range(devices)])  115 us
    ppermute x32, waiting for transfers between devices, turned(): lax.ppermute(x, axis, [(i, (i + by) % devices) for i in range(devices)])  62.9 us
    all_gather x1, waiting for transfers between devices, shards(): whole = lax.all_gather(mine, 'sp', axis=1, tiled=True)  60.5 us
    dot_general x48, matrix products, shards(): jnp.dot(scaled, rows_of(whole[4 * l + k], owner, width), preferred_elemen...  13.6 us
    dot_general x16, matrix products, shards(): jnp.dot(block, rows_of(whole[4 * l + 3], owner, width), preferred_element...  11.3 us
  transfers between devices with their start and end apart: 34, of which 20 were waited for; matrix products, arithmetic and copies ran while one was open for 7% of the time, Pallas kernels for 0%

profile of v1, /device:TPU:80, one launch (start us, length us, event | category | flops | bytes accessed | tf_op | source)
XLA Modules:
  0.0 299.8 jit_solution(8543728922268533358)
XLA Ops:
  14.1 1.8 collective-permute-start
  15.9 0.8 collective-permute-done
  16.7 1.0 constant_dynamic-update-slice_fusion
  17.7 3.6 %collective-permute-start.1 = (bf16[520,256]{1,0:T(8,128)(2,1)S(1)}, bf16[520,256]{1,0:T(8,128)(2,1)S(1)}, u32[]{:S(2)}, u32[]{:S(2)}) collective-permute-start(bf16[520,256]{1,0:T(8,128)(2,1)S(1)} %constant_dynamic-update-slice_fusion), channel_id=1, source_target_pairs={{0,1},{1,2},{2,3},{3,4},{4,5},{5,6},{6,7},{7,0},{8,9},{9,10},{10,1... | collective-permute-start | bytes 798728 | tf_op jit(solution)/shard_map/ppermute | solution.py:20
  21.3 4.1 %collective-permute-start.2 = (bf16[520,256]{1,0:T(8,128)(2,1)S(1)}, bf16[520,256]{1,0:T(8,128)(2,1)S(1)}, u32[]{:S(2)}, u32[]{:S(2)}) collective-permute-start(bf16[520,256]{1,0:T(8,128)(2,1)S(1)} %constant_dynamic-update-slice_fusion), channel_id=1, source_target_pairs={{0,7},{1,0},{2,1},{3,2},{4,3},{5,4},{6,5},{7,6},{8,15},{9,8},{10,9... | collective-permute-start | bytes 798728 | tf_op jit(solution)/shard_map/ppermute | solution.py:20
  25.4 0.8 slice_reduce_fusion.1
  27.1 2.5 collective-permute-done.2
  29.6 5.3 %collective-permute-start.4 = (bf16[520,256]{1,0:T(8,128)(2,1)S(1)}, bf16[520,256]{1,0:T(8,128)(2,1)S(1)}, u32[]{:S(2)}, u32[]{:S(2)}) collective-permute-start(bf16[520,256]{1,0:T(8,128)(2,1)S(1)} %collective-permute-done.2), channel_id=1, source_target_pairs={{0,7},{1,0},{2,1},{3,2},{4,3},{5,4},{6,5},{7,6},{8,15},{9,8},{10,9... | collective-permute-start | bytes 798728 | tf_op jit(solution)/shard_map/ppermute | solution.py:20
  35.0 2.0 collective-permute-start.3
  37.4 2.2 collective-permute-done.4
  39.6 5.6 %collective-permute-start.6 = (bf16[520,256]{1,0:T(8,128)(2,1)S(1)}, bf16[520,256]{1,0:T(8,128)(2,1)S(1)}, u32[]{:S(2)}, u32[]{:S(2)}) collective-permute-start(bf16[520,256]{1,0:T(8,128)(2,1)S(1)} %collective-permute-done.4), channel_id=1, source_target_pairs={{0,7},{1,0},{2,1},{3,2},{4,3},{5,4},{6,5},{7,6},{8,15},{9,8},{10,9... | collective-permute-start | bytes 798728 | tf_op jit(solution)/shard_map/ppermute | solution.py:20
  45.5 1.9 collective-permute-start.5
  48.0 3.0 %collective-permute-done.6 = bf16[520,256]{1,0:T(8,128)(2,1)S(1)} collective-permute-done((bf16[520,256]{1,0:T(8,128)(2,1)S(1)}, bf16[520,256]{1,0:T(8,128)(2,1)S(1)}, u32[]{:S(2)}, u32[]{:S(2)}) %collective-permute-start.6) | collective-permute-done | bytes 266272 | tf_op jit(solution)/shard_map/ppermute | solution.py:20
  51.1 5.6 %collective-permute-start.8 = (bf16[264,256]{1,0:T(8,128)(2,1)S(1)}, bf16[264,256]{1,0:T(8,128)(2,1)S(1)}, u32[]{:S(2)}, u32[]{:S(2)}) collective-permute-start(bf16[264,256]{1,0:T(8,128)(2,1)S(1)} %slice.224), channel_id=1, source_target_pairs={{0,7},{1,0},{2,1},{3,2},{4,3},{5,4},{6,5},{7,6},{8,15},{9,8},{10,9... | collective-permute-start | bytes 405512 | tf_op jit(solution)/shard_map/ppermute | solution.py:20
  57.3 2.0 collective-permute-start.7
  59.6 6.7 %collective-permute-done.7 = bf16[256,256]{1,0:T(8,128)(2,1)S(1)} collective-permute-done((bf16[256,256]{1,0:T(8,128)(2,1)S(1)}, bf16[256,256]{1,0:T(8,128)(2,1)S(1)}, u32[]{:S(2)}, u32[]{:S(2)}) %collective-permute-start.7) | collective-permute-done | bytes 131104 | tf_op jit(solution)/shard_map/ppermute | solution.py:20
  66.5 60.5 %all-gather.2.cloned.1.call-done = bf16[8,2048,256]{2,1,0:T(8,128)(2,1)} async-done(((bf16[8,64,256]{2,1,0:T(8,128)(2,1)}), bf16[8,2048,256]{2,1,0:T(8,128)(2,1)}) %all-gather.2.cloned.1.call-update) | async-done | bytes 8388624 | tf_op jit(solution)/shard_map/all_gather | solution.py:63
  127.0 5.5 %fusion.381 = (bf16[1,2048,256]{2,1,0:T(8,128)(2,1)S(1)}, bf16[1,2048,256]{2,1,0:T(8,128)(2,1)}, bf16[1,2048,256]{2,1,0:T(8,128)(2,1)}, bf16[1,2048,256]{2,1,0:T...) fusion(bf16[8,2048,256]{2,1,0:T(8,128)(2,1)} %all-gather.2.clon, ...), kind=kLoop, calls=%fused_computation.437 | loop fusion | bytes 16777216 | tf_op jit(solution)/shard_map/slice | solution.py:83
  138.3 1.1 fusion.48
  139.4 4.6 %collective-permute-start.10 = (bf16[520,256]{1,0:T(8,128)(2,1)}, bf16[520,256]{1,0:T(8,128)(2,1)}, u32[]{:S(2)}, u32[]{:S(2)}) collective-permute-start(bf16[520,256]{1,0:T(8,128)(2,1)} %fusion.48), channel_id=1, source_target_pairs={{0,7},{1,0},{2,1},{3,2},{4,3},{5,4},{6,5},{7,6},{8,15},{9,8},{10,9... | collective-permute-start | bytes 798728 | tf_op jit(solution)/shard_map/ppermute | solution.py:20
  144.1 2.1 collective-permute-start.9
  146.2 4.2 %collective-permute-done.10 = bf16[520,256]{1,0:T(8,128)(2,1)} collective-permute-done((bf16[520,256]{1,0:T(8,128)(2,1)}, bf16[520,256]{1,0:T(8,128)(2,1)}, u32[]{:S(2)}, u32[]{:S(2)}) %collective-permute-start.10) | collective-permute-done | bytes 266272 | tf_op jit(solution)/shard_map/ppermute | solution.py:20
  150.4 5.6 %collective-permute-start.12 = (bf16[520,256]{1,0:T(8,128)(2,1)}, bf16[520,256]{1,0:T(8,128)(2,1)S(1)}, u32[]{:S(2)}, u32[]{:S(2)}) collective-permute-start(bf16[520,256]{1,0:T(8,128)(2,1)} %collective-permute-done.10), channel_id=1, source_target_pairs={{0,7},{1,0},{2,1},{3,2},{4,3},{5,4},{6,5},{7,6},{8,15},{9,8},{10,9... | collective-permute-start | bytes 798728 | tf_op jit(solution)/shard_map/ppermute | solution.py:20
  156.0 1.2 fusion.206
  157.2 1.1 fusion.208
  158.4 2.0 collective-permute-start.11
  160.4 1.2 fusion.17
  161.6 5.4 %collective-permute-start.14 = (bf16[520,256]{1,0:T(8,128)(2,1)S(1)}, bf16[520,256]{1,0:T(8,128)(2,1)S(1)}, u32[]{:S(2)}, u32[]{:S(2)}) collective-permute-start(bf16[520,256]{1,0:T(8,128)(2,1)S(1)} %collective-permute-done.12), channel_id=1, source_target_pairs={{0,7},{1,0},{2,1},{3,2},{4,3},{5,4},{6,5},{7,6},{8,15},{9,8},{10,9... | collective-permute-start | bytes 798728 | tf_op jit(solution)/shard_map/ppermute | solution.py:20
  167.0 1.1 fusion.203
  168.9 1.9 collective-permute-start.13
  170.9 1.2 fusion.15
  172.1 5.2 %collective-permute-start.16 = (bf16[264,256]{1,0:T(8,128)(2,1)S(1)}, bf16[264,256]{1,0:T(8,128)(2,1)S(1)}, u32[]{:S(2)}, u32[]{:S(2)}) collective-permute-start(bf16[264,256]{1,0:T(8,128)(2,1)S(1)} %slice.229), channel_id=1, source_target_pairs={{0,7},{1,0},{2,1},{3,2},{4,3},{5,4},{6,5},{7,6},{8,15},{9,8},{10,9... | collective-permute-start | bytes 405512 | tf_op jit(solution)/shard_map/ppermute | solution.py:20
  177.2 1.3 collective-permute-done.13
  178.6 2.0 collective-permute-start.15
  180.5 1.1 fusion.200
  181.7 5.0 %collective-permute-done.15 = bf16[256,256]{1,0:T(8,128)(2,1)S(1)} collective-permute-done((bf16[256,256]{1,0:T(8,128)(2,1)S(1)}, bf16[256,256]{1,0:T(8,128)(2,1)S(1)}, u32[]{:S(2)}, u32[]{:S(2)}) %collective-permute-start.15) | collective-permute-done | bytes 131104 | tf_op jit(solution)/shard_map/ppermute | solution.py:20
  186.7 1.1 fusion.82
  187.8 1.3 fusion.80
  189.1 1.9 collective-permute-start.17
  191.1 5.2 %collective-permute-start.18 = (bf16[520,256]{1,0:T(8,128)(2,1)S(1)}, bf16[520,256]{1,0:T(8,128)(2,1)S(1)}, u32[]{:S(2)}, u32[]{:S(2)}) collective-permute-start(bf16[520,256]{1,0:T(8,128)(2,1)S(1)} %get-tuple-element.38), channel_id=1, source_target_pairs={{0,7},{1,0},{2,1},{3,2},{4,3},{5,4},{6,5},{7,6},{8,15},{9,8},{10,9... | collective-permute-start | bytes 798728 | tf_op jit(solution)/shard_map/ppermute | solution.py:20
  196.3 1.1 fusion.92
  197.9 2.3 collective-permute-done.18
  200.2 5.6 %collective-permute-start.20 = (bf16[520,256]{1,0:T(8,128)(2,1)S(1)}, bf16[520,256]{1,0:T(8,128)(2,1)S(1)}, u32[]{:S(2)}, u32[]{:S(2)}) collective-permute-start(bf16[520,256]{1,0:T(8,128)(2,1)S(1)} %collective-permute-done.18), channel_id=1, source_target_pairs={{0,7},{1,0},{2,1},{3,2},{4,3},{5,4},{6,5},{7,6},{8,15},{9,8},{10,9... | collective-permute-start | bytes 798728 | tf_op jit(solution)/shard_map/ppermute | solution.py:20
  205.8 2.0 collective-permute-start.19
  209.7 6.6 %collective-permute-done.19 = bf16[520,256]{1,0:T(8,128)(2,1)S(1)} collective-permute-done((bf16[520,256]{1,0:T(8,128)(2,1)S(1)}, bf16[520,256]{1,0:T(8,128)(2,1)S(1)}, u32[]{:S(2)}, u32[]{:S(2)}) %collective-permute-start.19) | collective-permute-done | bytes 266272 | tf_op jit(solution)/shard_map/ppermute | solution.py:20
  216.3 1.9 collective-permute-start.21
  218.4 5.3 %collective-permute-start.22 = (bf16[520,256]{1,0:T(8,128)(2,1)S(1)}, bf16[520,256]{1,0:T(8,128)(2,1)S(1)}, u32[]{:S(2)}, u32[]{:S(2)}) collective-permute-start(bf16[520,256]{1,0:T(8,128)(2,1)S(1)} %collective-permute-done.20), channel_id=1, source_target_pairs={{0,7},{1,0},{2,1},{3,2},{4,3},{5,4},{6,5},{7,6},{8,15},{9,8},{10,9... | collective-permute-start | bytes 798728 | tf_op jit(solution)/shard_map/ppermute | solution.py:20
  225.4 3.1 %collective-permute-done.22 = bf16[520,256]{1,0:T(8,128)(2,1)S(1)} collective-permute-done((bf16[520,256]{1,0:T(8,128)(2,1)S(1)}, bf16[520,256]{1,0:T(8,128)(2,1)S(1)}, u32[]{:S(2)}, u32[]{:S(2)}) %collective-permute-start.22) | collective-permute-done | bytes 266272 | tf_op jit(solution)/shard_map/ppermute | solution.py:20
  228.6 5.6 %collective-permute-start.24 = (bf16[264,256]{1,0:T(8,128)(2,1)S(1)}, bf16[264,256]{1,0:T(8,128)(2,1)S(1)}, u32[]{:S(2)}, u32[]{:S(2)}) collective-permute-start(bf16[264,256]{1,0:T(8,128)(2,1)S(1)} %slice.232), channel_id=1, source_target_pairs={{0,7},{1,0},{2,1},{3,2},{4,3},{5,4},{6,5},{7,6},{8,15},{9,8},{10,9... | collective-permute-start | bytes 405512 | tf_op jit(solution)/shard_map/ppermute | solution.py:20
  234.2 2.0 collective-permute-start.23
  237.3 6.5 %collective-permute-done.23 = bf16[256,256]{1,0:T(8,128)(2,1)S(1)} collective-permute-done((bf16[256,256]{1,0:T(8,128)(2,1)S(1)}, bf16[256,256]{1,0:T(8,128)(2,1)S(1)}, u32[]{:S(2)}, u32[]{:S(2)}) %collective-permute-start.23) | collective-permute-done | bytes 131104 | tf_op jit(solution)/shard_map/ppermute | solution.py:20
  245.6 2.0 collective-permute-start.26
  247.6 4.0 %collective-permute-start.25 = (bf16[520,256]{1,0:T(8,128)(2,1)S(1)}, bf16[520,256]{1,0:T(8,128)(2,1)S(1)}, u32[]{:S(2)}, u32[]{:S(2)}) collective-permute-start(bf16[520,256]{1,0:T(8,128)(2,1)S(1)} %fusion.47), channel_id=1, source_target_pairs={{0,1},{1,2},{2,3},{3,4},{4,5},{5,6},{6,7},{7,0},{8,9},{9,10},{10,1... | collective-permute-start | bytes 798728 | tf_op jit(solution)/shard_map/ppermute | solution.py:20
  251.8 2.2 collective-permute-done.26
  254.0 3.1 %collective-permute-start.28 = (bf16[520,256]{1,0:T(8,128)(2,1)S(1)}, bf16[520,256]{1,0:T(8,128)(2,1)S(1)}, u32[]{:S(2)}, u32[]{:S(2)}) collective-permute-start(bf16[520,256]{1,0:T(8,128)(2,1)S(1)} %collective-permute-done.26), channel_id=1, source_target_pairs={{0,7},{1,0},{2,1},{3,2},{4,3},{5,4},{6,5},{7,6},{8,15},{9,8},{10,9... | collective-permute-start | bytes 798728 | tf_op jit(solution)/shard_map/ppermute | solution.py:20
  257.4 2.7 collective-permute-start.27
  260.4 6.5 %collective-permute-done.27 = bf16[520,256]{1,0:T(8,128)(2,1)S(1)} collective-permute-done((bf16[520,256]{1,0:T(8,128)(2,1)S(1)}, bf16[520,256]{1,0:T(8,128)(2,1)S(1)}, u32[]{:S(2)}, u32[]{:S(2)}) %collective-permute-start.27) | collective-permute-done | bytes 266272 | tf_op jit(solution)/shard_map/ppermute | solution.py:20
  266.9 1.9 collective-permute-start.29
  268.9 5.2 %collective-permute-start.30 = (bf16[520,256]{1,0:T(8,128)(2,1)S(1)}, bf16[520,256]{1,0:T(8,128)(2,1)S(1)}, u32[]{:S(2)}, u32[]{:S(2)}) collective-permute-start(bf16[520,256]{1,0:T(8,128)(2,1)S(1)} %collective-permute-done.28), channel_id=1, source_target_pairs={{0,7},{1,0},{2,1},{3,2},{4,3},{5,4},{6,5},{7,6},{8,15},{9,8},{10,9... | collective-permute-start | bytes 798728 | tf_op jit(solution)/shard_map/ppermute | solution.py:20
  274.5 3.4 %collective-permute-done.30 = bf16[520,256]{1,0:T(8,128)(2,1)S(1)} collective-permute-done((bf16[520,256]{1,0:T(8,128)(2,1)S(1)}, bf16[520,256]{1,0:T(8,128)(2,1)S(1)}, u32[]{:S(2)}, u32[]{:S(2)}) %collective-permute-start.30) | collective-permute-done | bytes 266272 | tf_op jit(solution)/shard_map/ppermute | solution.py:20
  278.0 5.6 %collective-permute-start.32 = (bf16[264,256]{1,0:T(8,128)(2,1)S(1)}, bf16[264,256]{1,0:T(8,128)(2,1)S(1)}, u32[]{:S(2)}, u32[]{:S(2)}) collective-permute-start(bf16[264,256]{1,0:T(8,128)(2,1)S(1)} %slice.237), channel_id=1, source_target_pairs={{0,7},{1,0},{2,1},{3,2},{4,3},{5,4},{6,5},{7,6},{8,15},{9,8},{10,9... | collective-permute-start | bytes 405512 | tf_op jit(solution)/shard_map/ppermute | solution.py:20
  283.6 2.0 collective-permute-start.31
  286.1 5.7 %collective-permute-done.31 = bf16[256,256]{1,0:T(8,128)(2,1)S(1)} collective-permute-done((bf16[256,256]{1,0:T(8,128)(2,1)S(1)}, bf16[256,256]{1,0:T(8,128)(2,1)S(1)}, u32[]{:S(2)}, u32[]{:S(2)}) %collective-permute-start.31) | collective-permute-done | bytes 131104 | tf_op jit(solution)/shard_map/ppermute | solution.py:20
  292.0 0.9 fusion.81
  (121 shorter events, 26.0 us)
Async XLA Ops:
  6.5 120.5 %all-gather.2.cloned.1.call-start = ((), (), s32[]{:S(2)}) async-start(), calls=%async_computation | async-start | bytes 8650752 | tf_op jit(solution)/shard_map/all_gather | solution.py:63
  12.6 0.7 copy-start.3
  14.1 2.6 collective-permute-start
  17.7 17.3 %collective-permute-start.1 = (bf16[520,256]{1,0:T(8,128)(2,1)S(1)}, bf16[520,256]{1,0:T(8,128)(2,1)S(1)}, u32[]{:S(2)}, u32[]{:S(2)}) collective-permute-start(bf16[520,256]{1,0:T(8,128)(2,1)S(1)} %constant_dynamic-update-slice_fusion), channel_id=1, source_target_pairs={{0,1},{1,2},{2,3},{3,4},{4,5},{5,6},{6,7},{7,0},{8,9},{9,10},{10,1... | collective-permute-start | bytes 798728 | tf_op jit(solution)/shard_map/ppermute | solution.py:20
  21.3 8.3 %collective-permute-start.2 = (bf16[520,256]{1,0:T(8,128)(2,1)S(1)}, bf16[520,256]{1,0:T(8,128)(2,1)S(1)}, u32[]{:S(2)}, u32[]{:S(2)}) collective-permute-start(bf16[520,256]{1,0:T(8,128)(2,1)S(1)} %constant_dynamic-update-slice_fusion), channel_id=1, source_target_pairs={{0,7},{1,0},{2,1},{3,2},{4,3},{5,4},{6,5},{7,6},{8,15},{9,8},{10,9... | collective-permute-start | bytes 798728 | tf_op jit(solution)/shard_map/ppermute | solution.py:20
  29.6 10.0 %collective-permute-start.4 = (bf16[520,256]{1,0:T(8,128)(2,1)S(1)}, bf16[520,256]{1,0:T(8,128)(2,1)S(1)}, u32[]{:S(2)}, u32[]{:S(2)}) collective-permute-start(bf16[520,256]{1,0:T(8,128)(2,1)S(1)} %collective-permute-done.2), channel_id=1, source_target_pairs={{0,7},{1,0},{2,1},{3,2},{4,3},{5,4},{6,5},{7,6},{8,15},{9,8},{10,9... | collective-permute-start | bytes 798728 | tf_op jit(solution)/shard_map/ppermute | solution.py:20
  35.0 10.6 %collective-permute-start.3 = (bf16[520,256]{1,0:T(8,128)(2,1)S(1)}, bf16[520,256]{1,0:T(8,128)(2,1)S(1)}, u32[]{:S(2)}, u32[]{:S(2)}) collective-permute-start(bf16[520,256]{1,0:T(8,128)(2,1)S(1)} %collective-permute-done.1), channel_id=1, source_target_pairs={{0,1},{1,2},{2,3},{3,4},{4,5},{5,6},{6,7},{7,0},{8,9},{9,10},{10,1... | collective-permute-start | bytes 798728 | tf_op jit(solution)/shard_map/ppermute | solution.py:20
  39.6 11.4 %collective-permute-start.6 = (bf16[520,256]{1,0:T(8,128)(2,1)S(1)}, bf16[520,256]{1,0:T(8,128)(2,1)S(1)}, u32[]{:S(2)}, u32[]{:S(2)}) collective-permute-start(bf16[520,256]{1,0:T(8,128)(2,1)S(1)} %collective-permute-done.4), channel_id=1, source_target_pairs={{0,7},{1,0},{2,1},{3,2},{4,3},{5,4},{6,5},{7,6},{8,15},{9,8},{10,9... | collective-permute-start | bytes 798728 | tf_op jit(solution)/shard_map/ppermute | solution.py:20
  45.5 11.7 %collective-permute-start.5 = (bf16[520,256]{1,0:T(8,128)(2,1)S(1)}, bf16[520,256]{1,0:T(8,128)(2,1)S(1)}, u32[]{:S(2)}, u32[]{:S(2)}) collective-permute-start(bf16[520,256]{1,0:T(8,128)(2,1)S(1)} %collective-permute-done.3), channel_id=1, source_target_pairs={{0,1},{1,2},{2,3},{3,4},{4,5},{5,6},{6,7},{7,0},{8,9},{9,10},{10,1... | collective-permute-start | bytes 798728 | tf_op jit(solution)/shard_map/ppermute | solution.py:20
  51.1 15.3 %collective-permute-start.8 = (bf16[264,256]{1,0:T(8,128)(2,1)S(1)}, bf16[264,256]{1,0:T(8,128)(2,1)S(1)}, u32[]{:S(2)}, u32[]{:S(2)}) collective-permute-start(bf16[264,256]{1,0:T(8,128)(2,1)S(1)} %slice.224), channel_id=1, source_target_pairs={{0,7},{1,0},{2,1},{3,2},{4,3},{5,4},{6,5},{7,6},{8,15},{9,8},{10,9... | collective-permute-start | bytes 405512 | tf_op jit(solution)/shard_map/ppermute | solution.py:20
  57.3 9.0 %collective-permute-start.7 = (bf16[256,256]{1,0:T(8,128)(2,1)S(1)}, bf16[256,256]{1,0:T(8,128)(2,1)S(1)}, u32[]{:S(2)}, u32[]{:S(2)}) collective-permute-start(bf16[256,256]{1,0:T(8,128)(2,1)S(1)} %slice.223), channel_id=1, source_target_pairs={{0,1},{1,2},{2,3},{3,4},{4,5},{5,6},{6,7},{7,0},{8,9},{9,10},{10,1... | collective-permute-start | bytes 393224 | tf_op jit(solution)/shard_map/ppermute | solution.py:20
  138.3 59.4 %copy-start = (bf16[1,2048,256]{2,1,0:T(8,128)(2,1)S(1)}, bf16[1,2048,256]{2,1,0:T(8,128)(2,1)}, u32[]{:S(2)}) copy-start(bf16[1,2048,256]{2,1,0:T(8,128)(2,1)} %get-tuple-element.10) | copy-start | bytes 3145732
  139.4 68.4 %copy-start.1 = (bf16[1,2048,256]{2,1,0:T(8,128)(2,1)S(1)}, bf16[1,2048,256]{2,1,0:T(8,128)(2,1)}, u32[]{:S(2)}) copy-start(bf16[1,2048,256]{2,1,0:T(8,128)(2,1)} %get-tuple-element.9) | copy-start | bytes 3145732
  139.4 11.0 %collective-permute-start.10 = (bf16[520,256]{1,0:T(8,128)(2,1)}, bf16[520,256]{1,0:T(8,128)(2,1)}, u32[]{:S(2)}, u32[]{:S(2)}) collective-permute-start(bf16[520,256]{1,0:T(8,128)(2,1)} %fusion.48), channel_id=1, source_target_pairs={{0,7},{1,0},{2,1},{3,2},{4,3},{5,4},{6,5},{7,6},{8,15},{9,8},{10,9... | collective-permute-start | bytes 798728 | tf_op jit(solution)/shard_map/ppermute | solution.py:20
  144.1 53.3 %copy-start.2 = (bf16[1,2048,256]{2,1,0:T(8,128)(2,1)S(1)}, bf16[1,2048,256]{2,1,0:T(8,128)(2,1)}, u32[]{:S(2)}) copy-start(bf16[1,2048,256]{2,1,0:T(8,128)(2,1)} %get-tuple-element.8) | copy-start | bytes 3145732
  144.1 13.2 %collective-permute-start.9 = (bf16[520,256]{1,0:T(8,128)(2,1)}, bf16[520,256]{1,0:T(8,128)(2,1)S(1)}, u32[]{:S(2)}, u32[]{:S(2)}) collective-permute-start(bf16[520,256]{1,0:T(8,128)(2,1)} %fusion.48), channel_id=1, source_target_pairs={{0,1},{1,2},{2,3},{3,4},{4,5},{5,6},{6,7},{7,0},{8,9},{9,10},{10,1... | collective-permute-start | bytes 798728 | tf_op jit(solution)/shard_map/ppermute | solution.py:20
  150.4 11.2 %collective-permute-start.12 = (bf16[520,256]{1,0:T(8,128)(2,1)}, bf16[520,256]{1,0:T(8,128)(2,1)S(1)}, u32[]{:S(2)}, u32[]{:S(2)}) collective-permute-start(bf16[520,256]{1,0:T(8,128)(2,1)} %collective-permute-done.10), channel_id=1, source_target_pairs={{0,7},{1,0},{2,1},{3,2},{4,3},{5,4},{6,5},{7,6},{8,15},{9,8},{10,9... | collective-permute-start | bytes 798728 | tf_op jit(solution)/shard_map/ppermute | solution.py:20
  158.4 10.5 %collective-permute-start.11 = (bf16[520,256]{1,0:T(8,128)(2,1)S(1)}, bf16[520,256]{1,0:T(8,128)(2,1)S(1)}, u32[]{:S(2)}, u32[]{:S(2)}) collective-permute-start(bf16[520,256]{1,0:T(8,128)(2,1)S(1)} %collective-permute-done.9), channel_id=1, source_target_pairs={{0,1},{1,2},{2,3},{3,4},{4,5},{5,6},{6,7},{7,0},{8,9},{9,10},{10,1... | collective-permute-start | bytes 798728 | tf_op jit(solution)/shard_map/ppermute | solution.py:20
  161.6 10.4 %collective-permute-start.14 = (bf16[520,256]{1,0:T(8,128)(2,1)S(1)}, bf16[520,256]{1,0:T(8,128)(2,1)S(1)}, u32[]{:S(2)}, u32[]{:S(2)}) collective-permute-start(bf16[520,256]{1,0:T(8,128)(2,1)S(1)} %collective-permute-done.12), channel_id=1, source_target_pairs={{0,7},{1,0},{2,1},{3,2},{4,3},{5,4},{6,5},{7,6},{8,15},{9,8},{10,9... | collective-permute-start | bytes 798728 | tf_op jit(solution)/shard_map/ppermute | solution.py:20
  168.9 9.7 %collective-permute-start.13 = (bf16[520,256]{1,0:T(8,128)(2,1)S(1)}, bf16[520,256]{1,0:T(8,128)(2,1)S(1)}, u32[]{:S(2)}, u32[]{:S(2)}) collective-permute-start(bf16[520,256]{1,0:T(8,128)(2,1)S(1)} %collective-permute-done.11), channel_id=1, source_target_pairs={{0,1},{1,2},{2,3},{3,4},{4,5},{5,6},{6,7},{7,0},{8,9},{9,10},{10,1... | collective-permute-start | bytes 798728 | tf_op jit(solution)/shard_map/ppermute | solution.py:20
  172.1 14.6 %collective-permute-start.16 = (bf16[264,256]{1,0:T(8,128)(2,1)S(1)}, bf16[264,256]{1,0:T(8,128)(2,1)S(1)}, u32[]{:S(2)}, u32[]{:S(2)}) collective-permute-start(bf16[264,256]{1,0:T(8,128)(2,1)S(1)} %slice.229), channel_id=1, source_target_pairs={{0,7},{1,0},{2,1},{3,2},{4,3},{5,4},{6,5},{7,6},{8,15},{9,8},{10,9... | collective-permute-start | bytes 405512 | tf_op jit(solution)/shard_map/ppermute | solution.py:20
  178.6 8.1 %collective-permute-start.15 = (bf16[256,256]{1,0:T(8,128)(2,1)S(1)}, bf16[256,256]{1,0:T(8,128)(2,1)S(1)}, u32[]{:S(2)}, u32[]{:S(2)}) collective-permute-start(bf16[256,256]{1,0:T(8,128)(2,1)S(1)} %slice.228), channel_id=1, source_target_pairs={{0,1},{1,2},{2,3},{3,4},{4,5},{5,6},{6,7},{7,0},{8,9},{9,10},{10,1... | collective-permute-start | bytes 393224 | tf_op jit(solution)/shard_map/ppermute | solution.py:20
  189.1 16.7 %collective-permute-start.17 = (bf16[520,256]{1,0:T(8,128)(2,1)S(1)}, bf16[520,256]{1,0:T(8,128)(2,1)S(1)}, u32[]{:S(2)}, u32[]{:S(2)}) collective-permute-start(bf16[520,256]{1,0:T(8,128)(2,1)S(1)} %get-tuple-element.38), channel_id=1, source_target_pairs={{0,1},{1,2},{2,3},{3,4},{4,5},{5,6},{6,7},{7,0},{8,9},{9,10},{10,1... | collective-permute-start | bytes 798728 | tf_op jit(solution)/shard_map/ppermute | solution.py:20
  191.1 9.1 %collective-permute-start.18 = (bf16[520,256]{1,0:T(8,128)(2,1)S(1)}, bf16[520,256]{1,0:T(8,128)(2,1)S(1)}, u32[]{:S(2)}, u32[]{:S(2)}) collective-permute-start(bf16[520,256]{1,0:T(8,128)(2,1)S(1)} %get-tuple-element.38), channel_id=1, source_target_pairs={{0,7},{1,0},{2,1},{3,2},{4,3},{5,4},{6,5},{7,6},{8,15},{9,8},{10,9... | collective-permute-start | bytes 798728 | tf_op jit(solution)/shard_map/ppermute | solution.py:20
  200.2 18.2 %collective-permute-start.20 = (bf16[520,256]{1,0:T(8,128)(2,1)S(1)}, bf16[520,256]{1,0:T(8,128)(2,1)S(1)}, u32[]{:S(2)}, u32[]{:S(2)}) collective-permute-start(bf16[520,256]{1,0:T(8,128)(2,1)S(1)} %collective-permute-done.18), channel_id=1, source_target_pairs={{0,7},{1,0},{2,1},{3,2},{4,3},{5,4},{6,5},{7,6},{8,15},{9,8},{10,9... | collective-permute-start | bytes 798728 | tf_op jit(solution)/shard_map/ppermute | solution.py:20
  205.8 10.5 %collective-permute-start.19 = (bf16[520,256]{1,0:T(8,128)(2,1)S(1)}, bf16[520,256]{1,0:T(8,128)(2,1)S(1)}, u32[]{:S(2)}, u32[]{:S(2)}) collective-permute-start(bf16[520,256]{1,0:T(8,128)(2,1)S(1)} %collective-permute-done.17), channel_id=1, source_target_pairs={{0,1},{1,2},{2,3},{3,4},{4,5},{5,6},{6,7},{7,0},{8,9},{9,10},{10,1... | collective-permute-start | bytes 798728 | tf_op jit(solution)/shard_map/ppermute | solution.py:20
  216.3 17.9 %collective-permute-start.21 = (bf16[520,256]{1,0:T(8,128)(2,1)S(1)}, bf16[520,256]{1,0:T(8,128)(2,1)S(1)}, u32[]{:S(2)}, u32[]{:S(2)}) collective-permute-start(bf16[520,256]{1,0:T(8,128)(2,1)S(1)} %collective-permute-done.19), channel_id=1, source_target_pairs={{0,1},{1,2},{2,3},{3,4},{4,5},{5,6},{6,7},{7,0},{8,9},{9,10},{10,1... | collective-permute-start | bytes 798728 | tf_op jit(solution)/shard_map/ppermute | solution.py:20
  218.4 10.1 %collective-permute-start.22 = (bf16[520,256]{1,0:T(8,128)(2,1)S(1)}, bf16[520,256]{1,0:T(8,128)(2,1)S(1)}, u32[]{:S(2)}, u32[]{:S(2)}) collective-permute-start(bf16[520,256]{1,0:T(8,128)(2,1)S(1)} %collective-permute-done.20), channel_id=1, source_target_pairs={{0,7},{1,0},{2,1},{3,2},{4,3},{5,4},{6,5},{7,6},{8,15},{9,8},{10,9... | collective-permute-start | bytes 798728 | tf_op jit(solution)/shard_map/ppermute | solution.py:20
  228.6 15.2 %collective-permute-start.24 = (bf16[264,256]{1,0:T(8,128)(2,1)S(1)}, bf16[264,256]{1,0:T(8,128)(2,1)S(1)}, u32[]{:S(2)}, u32[]{:S(2)}) collective-permute-start(bf16[264,256]{1,0:T(8,128)(2,1)S(1)} %slice.232), channel_id=1, source_target_pairs={{0,7},{1,0},{2,1},{3,2},{4,3},{5,4},{6,5},{7,6},{8,15},{9,8},{10,9... | collective-permute-start | bytes 405512 | tf_op jit(solution)/shard_map/ppermute | solution.py:20
  234.2 9.5 %collective-permute-start.23 = (bf16[256,256]{1,0:T(8,128)(2,1)S(1)}, bf16[256,256]{1,0:T(8,128)(2,1)S(1)}, u32[]{:S(2)}, u32[]{:S(2)}) collective-permute-start(bf16[256,256]{1,0:T(8,128)(2,1)S(1)} %slice.231), channel_id=1, source_target_pairs={{0,1},{1,2},{2,3},{3,4},{4,5},{5,6},{6,7},{7,0},{8,9},{9,10},{10,1... | collective-permute-start | bytes 393224 | tf_op jit(solution)/shard_map/ppermute | solution.py:20
  245.6 8.3 %collective-permute-start.26 = (bf16[520,256]{1,0:T(8,128)(2,1)S(1)}, bf16[520,256]{1,0:T(8,128)(2,1)S(1)}, u32[]{:S(2)}, u32[]{:S(2)}) collective-permute-start(bf16[520,256]{1,0:T(8,128)(2,1)S(1)} %fusion.47), channel_id=1, source_target_pairs={{0,7},{1,0},{2,1},{3,2},{4,3},{5,4},{6,5},{7,6},{8,15},{9,8},{10,9... | collective-permute-start | bytes 798728 | tf_op jit(solution)/shard_map/ppermute | solution.py:20
  247.6 9.8 %collective-permute-start.25 = (bf16[520,256]{1,0:T(8,128)(2,1)S(1)}, bf16[520,256]{1,0:T(8,128)(2,1)S(1)}, u32[]{:S(2)}, u32[]{:S(2)}) collective-permute-start(bf16[520,256]{1,0:T(8,128)(2,1)S(1)} %fusion.47), channel_id=1, source_target_pairs={{0,1},{1,2},{2,3},{3,4},{4,5},{5,6},{6,7},{7,0},{8,9},{9,10},{10,1... | collective-permute-start | bytes 798728 | tf_op jit(solution)/shard_map/ppermute | solution.py:20
  254.0 14.9 %collective-permute-start.28 = (bf16[520,256]{1,0:T(8,128)(2,1)S(1)}, bf16[520,256]{1,0:T(8,128)(2,1)S(1)}, u32[]{:S(2)}, u32[]{:S(2)}) collective-permute-start(bf16[520,256]{1,0:T(8,128)(2,1)S(1)} %collective-permute-done.26), channel_id=1, source_target_pairs={{0,7},{1,0},{2,1},{3,2},{4,3},{5,4},{6,5},{7,6},{8,15},{9,8},{10,9... | collective-permute-start | bytes 798728 | tf_op jit(solution)/shard_map/ppermute | solution.py:20
  257.4 9.6 %collective-permute-start.27 = (bf16[520,256]{1,0:T(8,128)(2,1)S(1)}, bf16[520,256]{1,0:T(8,128)(2,1)S(1)}, u32[]{:S(2)}, u32[]{:S(2)}) collective-permute-start(bf16[520,256]{1,0:T(8,128)(2,1)S(1)} %collective-permute-done.25), channel_id=1, source_target_pairs={{0,1},{1,2},{2,3},{3,4},{4,5},{5,6},{6,7},{7,0},{8,9},{9,10},{10,1... | collective-permute-start | bytes 798728 | tf_op jit(solution)/shard_map/ppermute | solution.py:20
  266.9 16.7 %collective-permute-start.29 = (bf16[520,256]{1,0:T(8,128)(2,1)S(1)}, bf16[520,256]{1,0:T(8,128)(2,1)S(1)}, u32[]{:S(2)}, u32[]{:S(2)}) collective-permute-start(bf16[520,256]{1,0:T(8,128)(2,1)S(1)} %collective-permute-done.27), channel_id=1, source_target_pairs={{0,1},{1,2},{2,3},{3,4},{4,5},{5,6},{6,7},{7,0},{8,9},{9,10},{10,1... | collective-permute-start | bytes 798728 | tf_op jit(solution)/shard_map/ppermute | solution.py:20
  268.9 9.1 %collective-permute-start.30 = (bf16[520,256]{1,0:T(8,128)(2,1)S(1)}, bf16[520,256]{1,0:T(8,128)(2,1)S(1)}, u32[]{:S(2)}, u32[]{:S(2)}) collective-permute-start(bf16[520,256]{1,0:T(8,128)(2,1)S(1)} %collective-permute-done.28), channel_id=1, source_target_pairs={{0,7},{1,0},{2,1},{3,2},{4,3},{5,4},{6,5},{7,6},{8,15},{9,8},{10,9... | collective-permute-start | bytes 798728 | tf_op jit(solution)/shard_map/ppermute | solution.py:20
  278.0 13.8 %collective-permute-start.32 = (bf16[264,256]{1,0:T(8,128)(2,1)S(1)}, bf16[264,256]{1,0:T(8,128)(2,1)S(1)}, u32[]{:S(2)}, u32[]{:S(2)}) collective-permute-start(bf16[264,256]{1,0:T(8,128)(2,1)S(1)} %slice.237), channel_id=1, source_target_pairs={{0,7},{1,0},{2,1},{3,2},{4,3},{5,4},{6,5},{7,6},{8,15},{9,8},{10,9... | collective-permute-start | bytes 405512 | tf_op jit(solution)/shard_map/ppermute | solution.py:20
  283.6 8.1 %collective-permute-start.31 = (bf16[256,256]{1,0:T(8,128)(2,1)S(1)}, bf16[256,256]{1,0:T(8,128)(2,1)S(1)}, u32[]{:S(2)}, u32[]{:S(2)}) collective-permute-start(bf16[256,256]{1,0:T(8,128)(2,1)S(1)} %slice.236), channel_id=1, source_target_pairs={{0,1},{1,2},{2,3},{3,4},{4,5},{5,6},{6,7},{7,0},{8,9},{9,10},{10,1... | collective-permute-start | bytes 393224 | tf_op jit(solution)/shard_map/ppermute | solution.py:20
Sparse Core Ops, SparseCore 0:
  13.5 113.4 all-gather.1

commit v2 on v1

v2 whole, which is shorter than its diff:
```python
import jax
import jax.numpy as jnp
from jax import lax
from jax.sharding import PartitionSpec as P

EPS = 1e-06
TILE_ROWS = 8
CHUNKS = 2
F32 = jnp.float32
BF16 = jnp.bfloat16


def passed_along(x, axis, by):
    devices = lax.axis_size(axis)
    pairs = [(i, i + by) for i in range(devices) if 0 <= i + by < devices]
    return lax.ppermute(x, axis, pairs)


def swapped(x, step):
    lines, devices = lax.axis_size("sp"), lax.axis_size("tp")
    pairs = []
    for s in range(lines):
        for i in range(devices):
            to = i + 1 if i % 2 == (step + s) % 2 else i - 1
            pairs.append((s * devices + i, s * devices + to % devices))
    return lax.ppermute(x, ("sp", "tp"), pairs)


def arriving(block):
    devices = lax.axis_size("tp")
    me, line = lax.axis_index("tp"), lax.axis_index("sp")
    side = jnp.where(me % 2 == line % 2, 1, -1)
    rows = block.shape[0]

    def owner(k):
        return (me + k * side + devices) % devices

    pair = jnp.concatenate([block, swapped(block, 0)], axis=0)
    blocks = [(owner(0), pair[:rows]), (owner(1), pair[rows:])]
    for step in range(1, devices // 2):
        pair = swapped(pair, step)
        near = -step if step % 2 else step
        far = near - 1 if step % 2 else near + 1
        blocks += [(owner(near), pair[:rows]), (owner(far), pair[rows:])]
    return blocks


def rows_of(weight, owner, count):
    return lax.dynamic_slice_in_dim(weight, owner * count, count, axis=0)


def convolve(carried, tap_rows):
    reach = tap_rows.shape[0] - 1
    count = carried.shape[0]
    padded = jnp.concatenate([jnp.zeros((reach, carried.shape[1]), F32), carried], axis=0)
    result = jnp.zeros_like(carried)
    for tap in range(reach + 1):
        result = result + tap_rows[tap].astype(F32) * padded[tap : tap + count]
    return result


def shards(tokens, mix_gain, gate_weight, mix_weight, value_weight, out_weight, conv_taps):
    layers, _, width = gate_weight.shape
    devices = lax.axis_size("tp")
    reach = conv_taps.shape[1] - 1
    fringe = -(-reach * layers // TILE_ROWS) * TILE_ROWS
    before = passed_along(tokens[tokens.shape[0] - fringe :], "sp", 1)
    extended = jnp.concatenate([before, tokens], axis=0)
    count = tokens.shape[0] // CHUNKS
    streams = [extended[c * count : (c + 1) * count + fringe] for c in range(CHUNKS)]
    kinds = (gate_weight, mix_weight, value_weight, out_weight)
    whole = lax.all_gather(jnp.concatenate(kinds, axis=0), "sp", axis=1, tiled=True)

    for l in range(layers):
        gains = mix_gain[l].reshape(devices, 1, width)
        for c in range(CHUNKS):
            stream = streams[c]
            total = [0.0] * 3
            squares = 0.0
            for owner, block in arriving(stream):
                wide = block.astype(F32)
                squares = squares + jnp.sum(wide * wide, axis=1, keepdims=True)
                scaled = (wide * lax.dynamic_index_in_dim(gains, owner, 0, False).astype(F32)).astype(BF16)
                for k in range(3):
                    part = rows_of(whole[k * layers + l], owner, width)
                    total[k] = total[k] + jnp.dot(scaled, part, preferred_element_type=F32)
            factor = lax.rsqrt(squares / (devices * width) + EPS)
            gate, inner, values = ((t * factor).astype(BF16).astype(F32) for t in total)
            mixed = (gate * convolve(inner * values, conv_taps[l])).astype(BF16)
            product = stream.astype(F32)
            for owner, block in arriving(mixed):
                part = rows_of(whole[3 * layers + l], owner, width)
                product = product + jnp.dot(block, part, preferred_element_type=F32)
            streams[c] = product.astype(BF16)
    return jnp.concatenate([stream[fringe:] for stream in streams], axis=0)


def solution(mesh):
    return jax.shard_map(
        shards,
        mesh=mesh,
        in_specs=(
            P(("grp", "sp"), "tp"),
            P(),
            P(None, "sp", "tp"),
            P(None, "sp", "tp"),
            P(None, "sp", "tp"),
            P(None, "sp", "tp"),
            P(None, None, "tp"),
        ),
        out_specs=P(("grp", "sp"), "tp"),
        check_vma=False,
    )
```

time: 302 us -> 277 us (0.917)
  starting transfers between devices: 117 us -> 101 us
  local copies, waits for them, and re-layouts: 14.9 us -> 6.14 us
  waiting for transfers between devices: 124 us -> 119 us
  other arithmetic: 4.44 us -> 7.69 us
    ppermute x32, starting transfers between devices: 115 us -> 97.6 us  [swapped(): return lax.ppermute(x, ('sp', 'tp'), pairs)]
    ppermute x32, waiting for transfers between devices: 62.9 us -> 53 us  [swapped(): return lax.ppermute(x, ('sp', 'tp'), pairs)]
    unnamed x16 -> x2, local copies, waits for them, and re-layouts: 6.04 us -> 0.01 us
    all_gather x1, waiting for transfers between devices: 60.5 us -> 65.9 us  [shards(): lax.all_gather(jnp.concatenate(kinds, axis=0), 'sp', axis=1, tiled=True)]
    dot_general x64 -> x128, matrix products: 24.9 us -> 26 us  [the longest x96 19.4 us: shards(): total[k] = total[k] + jnp.dot(scaled, part, preferred_element_type=F32)]
  transfers between devices with their start and end apart: 34 -> 34, of which waited for: 20 -> 24; matrix products, arithmetic and copies ran while one was open for 7% -> 10% of each run, Pallas kernels for 0% -> 0%
where the time goes in v2:
time: 277 us; the launch traced here: 275 us
  waiting for transfers between devices  119 us (43%)
  starting transfers between devices  101 us (36%)
  matrix products  26 us (9%)
  between operations  15.1 us (5%)
  other arithmetic  7.69 us (3%)
  local copies, waits for them, and re-layouts  6.14 us (2%)
    ppermute x32, starting transfers between devices, swapped(): return lax.ppermute(x, ('sp', 'tp'), pairs)  97.6 us
    all_gather x1, waiting for transfers between devices, shards(): lax.all_gather(jnp.concatenate(kinds, axis=0), 'sp', axis=1, tiled=True)  65.9 us
    ppermute x32, waiting for transfers between devices, swapped(): return lax.ppermute(x, ('sp', 'tp'), pairs)  53 us
    dot_general x96, matrix products, shards(): total[k] = total[k] + jnp.dot(scaled, part, preferred_element_type=F32)  19.4 us
    dot_general x32, matrix products, shards(): product = product + jnp.dot(block, part, preferred_element_type=F32)  6.54 us
  transfers between devices with their start and end apart: 34, of which 24 were waited for; matrix products, arithmetic and copies ran while one was open for 10% of the time, Pallas kernels for 0%

profile of v2, /device:TPU:80, one launch (start us, length us, event | category | flops | bytes accessed | tf_op | source)
XLA Modules:
  0.0 275.2 jit_solution(2780357564396165202)
XLA Ops:
  6.6 1.7 pad_maximum_fusion.8
  8.3 0.9 slice.420
  9.2 3.6 %collective-permute-start.17 = (bf16[264,256]{1,0:T(8,128)(2,1)S(1)}, bf16[264,256]{1,0:T(8,128)(2,1)S(1)}, u32[]{:S(2)}, u32[]{:S(2)}) collective-permute-start(bf16[264,256]{1,0:T(8,128)(2,1)S(1)} %slice.420), channel_id=1, source_target_pairs={{0,1},{1,0},{2,3},{3,2},{4,5},{5,4},{6,7},{7,6},{8,15},{9,10},{10,... | collective-permute-start | bytes 405512 | tf_op jit(solution)/shard_map/ppermute | solution.py:26
  12.8 0.7 slice.166
  13.5 3.7 %collective-permute-start = (bf16[8,256]{1,0:T(8,128)(2,1)S(1)}, bf16[8,256]{1,0:T(8,128)(2,1)S(1)}, u32[]{:S(2)}, u32[]{:S(2)}) collective-permute-start(bf16[8,256]{1,0:T(8,128)(2,1)S(1)} %slice.166), channel_id=1, source_target_pairs={{0,8},{8,16},{16,24},{24,32},{32,40},{40,48},{48,56},{56,64},{64,7... | collective-permute-start | bytes 12296 | tf_op jit(solution)/shard_map/ppermute | solution.py:16
  17.3 0.8 slice_reduce_fusion
  18.1 0.8 slice_convert_fusion.2
  19.0 1.2 fusion.118
  20.2 2.0 collective-permute-start.1
  22.2 4.5 %collective-permute-start.18 = (bf16[528,256]{1,0:T(8,128)(2,1)S(1)}, bf16[528,256]{1,0:T(8,128)(2,1)S(1)}, u32[]{:S(2)}, u32[]{:S(2)}) collective-permute-start(bf16[528,256]{1,0:T(8,128)(2,1)S(1)} %pad_maximum_fusion.4), channel_id=1, source_target_pairs={{0,7},{1,2},{2,1},{3,4},{4,3},{5,6},{6,5},{7,0},{8,9},{9,8},{10,11... | collective-permute-start | bytes 811016 | tf_op jit(solution)/shard_map/ppermute | solution.py:26
  27.2 3.0 %collective-permute-start.2 = (bf16[528,256]{1,0:T(8,128)(2,1)S(1)}, bf16[528,256]{1,0:T(8,128)(2,1)S(1)}, u32[]{:S(2)}, u32[]{:S(2)}) collective-permute-start(bf16[528,256]{1,0:T(8,128)(2,1)S(1)} %pad_maximum_fusion), channel_id=1, source_target_pairs={{0,7},{1,2},{2,1},{3,4},{4,3},{5,6},{6,5},{7,0},{8,9},{9,8},{10,11... | collective-permute-start | bytes 811016 | tf_op jit(solution)/shard_map/ppermute | solution.py:26
  30.3 3.0 %collective-permute-done.18 = bf16[528,256]{1,0:T(8,128)(2,1)S(1)} collective-permute-done((bf16[528,256]{1,0:T(8,128)(2,1)S(1)}, bf16[528,256]{1,0:T(8,128)(2,1)S(1)}, u32[]{:S(2)}, u32[]{:S(2)}) %collective-permute-start.18) | collective-permute-done | bytes 270368 | tf_op jit(solution)/shard_map/ppermute | solution.py:26
  33.2 1.9 collective-permute-start.19
  35.5 1.3 collective-permute-done.2
  36.8 2.7 collective-permute-start.3
  39.6 2.6 collective-permute-done.19
  42.2 4.9 %collective-permute-start.20 = (bf16[528,256]{1,0:T(8,128)(2,1)S(1)}, bf16[528,256]{1,0:T(8,128)(2,1)S(1)}, u32[]{:S(2)}, u32[]{:S(2)}) collective-permute-start(bf16[528,256]{1,0:T(8,128)(2,1)S(1)} %collective-permute-done.19), channel_id=1, source_target_pairs={{0,7},{1,2},{2,1},{3,4},{4,3},{5,6},{6,5},{7,0},{8,9},{9,8},{10,11... | collective-permute-start | bytes 811016 | tf_op jit(solution)/shard_map/ppermute | solution.py:26
  47.5 2.5 collective-permute-start.4
  50.2 1.7 collective-permute-done.20
  52.1 5.0 %collective-permute-done.4 = bf16[528,256]{1,0:T(8,128)(2,1)S(1)} collective-permute-done((bf16[528,256]{1,0:T(8,128)(2,1)S(1)}, bf16[528,256]{1,0:T(8,128)(2,1)S(1)}, u32[]{:S(2)}, u32[]{:S(2)}) %collective-permute-start.4) | collective-permute-done | bytes 270368 | tf_op jit(solution)/shard_map/ppermute | solution.py:26
  57.3 65.9 %all-gather.2.cloned.1.call-done = bf16[8,2048,256]{2,1,0:T(8,128)(2,1)} async-done(((bf16[8,64,256]{2,1,0:T(8,128)(2,1)}), bf16[8,2048,256]{2,1,0:T(8,128)(2,1)}) %all-gather.2.cloned.1.call-update) | async-done | bytes 8388624 | tf_op jit(solution)/shard_map/all_gather | solution.py:72
  123.3 3.7 %fusion.683 = (bf16[1,2048,256]{2,1,0:T(8,128)(2,1)S(1)}, bf16[1,2048,256]{2,1,0:T(8,128)(2,1)S(1)}, bf16[1,2048,256]{2,1,0:T(8,128)(2,1)S(1)}, bf16[1,2048,256]...) fusion(bf16[8,2048,256]{2,1,0:T(8,128)(2,1)} %all-gather.2.clon, ...), kind=kLoop, calls=%fused_computation.795 | loop fusion | bytes 16777216 | tf_op jit(solution)/shard_map/slice | solution.py:92
  132.6 3.1 %collective-permute-start.21 = (bf16[264,256]{1,0:T(8,128)(2,1)S(1)}, bf16[264,256]{1,0:T(8,128)(2,1)S(1)}, u32[]{:S(2)}, u32[]{:S(2)}) collective-permute-start(bf16[264,256]{1,0:T(8,128)(2,1)S(1)} %fusion.45), channel_id=1, source_target_pairs={{0,1},{1,0},{2,3},{3,2},{4,5},{5,4},{6,7},{7,6},{8,15},{9,10},{10,... | collective-permute-start | bytes 405512 | tf_op jit(solution)/shard_map/ppermute | solution.py:26
  140.1 2.8 %collective-permute-start.5 = (bf16[264,256]{1,0:T(8,128)(2,1)S(1)}, bf16[264,256]{1,0:T(8,128)(2,1)S(1)}, u32[]{:S(2)}, u32[]{:S(2)}) collective-permute-start(bf16[264,256]{1,0:T(8,128)(2,1)S(1)} %fusion.26), channel_id=1, source_target_pairs={{0,1},{1,0},{2,3},{3,2},{4,5},{5,4},{6,7},{7,6},{8,15},{9,10},{10,... | collective-permute-start | bytes 405512 | tf_op jit(solution)/shard_map/ppermute | solution.py:26
  143.1 3.9 %collective-permute-done.5 = bf16[264,256]{1,0:T(8,128)(2,1)S(1)} collective-permute-done((bf16[264,256]{1,0:T(8,128)(2,1)S(1)}, bf16[264,256]{1,0:T(8,128)(2,1)S(1)}, u32[]{:S(2)}, u32[]{:S(2)}) %collective-permute-start.5) | collective-permute-done | bytes 135200 | tf_op jit(solution)/shard_map/ppermute | solution.py:26
  147.0 4.5 %collective-permute-start.6 = (bf16[528,256]{1,0:T(8,128)(2,1)S(1)}, bf16[528,256]{1,0:T(8,128)(2,1)S(1)}, u32[]{:S(2)}, u32[]{:S(2)}) collective-permute-start(bf16[528,256]{1,0:T(8,128)(2,1)S(1)} %pad_maximum_fusion.1), channel_id=1, source_target_pairs={{0,7},{1,2},{2,1},{3,4},{4,3},{5,6},{6,5},{7,0},{8,9},{9,8},{10,11... | collective-permute-start | bytes 811016 | tf_op jit(solution)/shard_map/ppermute | solution.py:26
  151.6 2.6 collective-permute-start.22
  154.4 2.2 collective-permute-done.6
  157.3 4.0 %collective-permute-done.22 = bf16[528,256]{1,0:T(8,128)(2,1)S(1)} collective-permute-done((bf16[528,256]{1,0:T(8,128)(2,1)S(1)}, bf16[528,256]{1,0:T(8,128)(2,1)S(1)}, u32[]{:S(2)}, u32[]{:S(2)}) %collective-permute-start.22) | collective-permute-done | bytes 270368 | tf_op jit(solution)/shard_map/ppermute | solution.py:26
  161.2 1.9 collective-permute-start.23
  163.6 4.0 %collective-permute-start.7 = (bf16[528,256]{1,0:T(8,128)(2,1)S(1)}, bf16[528,256]{1,0:T(8,128)(2,1)S(1)}, u32[]{:S(2)}, u32[]{:S(2)}) collective-permute-start(bf16[528,256]{1,0:T(8,128)(2,1)S(1)} %collective-permute-done.6), channel_id=1, source_target_pairs={{0,1},{1,0},{2,3},{3,2},{4,5},{5,4},{6,7},{7,6},{8,15},{9,10},{10,... | collective-permute-start | bytes 811016 | tf_op jit(solution)/shard_map/ppermute | solution.py:26
  167.8 1.8 collective-permute-done.23
  169.6 2.8 %collective-permute-start.24 = (bf16[528,256]{1,0:T(8,128)(2,1)S(1)}, bf16[528,256]{1,0:T(8,128)(2,1)S(1)}, u32[]{:S(2)}, u32[]{:S(2)}) collective-permute-start(bf16[528,256]{1,0:T(8,128)(2,1)S(1)} %collective-permute-done.23), channel_id=1, source_target_pairs={{0,7},{1,2},{2,1},{3,4},{4,3},{5,6},{6,5},{7,0},{8,9},{9,8},{10,11... | collective-permute-start | bytes 811016 | tf_op jit(solution)/shard_map/ppermute | solution.py:26
  172.6 0.6 collective-permute-done.7
  173.2 4.3 %collective-permute-start.8 = (bf16[528,256]{1,0:T(8,128)(2,1)S(1)}, bf16[528,256]{1,0:T(8,128)(2,1)S(1)}, u32[]{:S(2)}, u32[]{:S(2)}) collective-permute-start(bf16[528,256]{1,0:T(8,128)(2,1)S(1)} %collective-permute-done.7), channel_id=1, source_target_pairs={{0,7},{1,2},{2,1},{3,4},{4,3},{5,6},{6,5},{7,0},{8,9},{9,8},{10,11... | collective-permute-start | bytes 811016 | tf_op jit(solution)/shard_map/ppermute | solution.py:26
  178.2 1.0 collective-permute-done.24
  179.7 1.9 collective-permute-start.25
  181.9 2.3 collective-permute-done.8
  184.9 3.3 %collective-permute-start.9 = (bf16[264,256]{1,0:T(8,128)(2,1)S(1)}, bf16[264,256]{1,0:T(8,128)(2,1)S(1)}, u32[]{:S(2)}, u32[]{:S(2)}) collective-permute-start(bf16[264,256]{1,0:T(8,128)(2,1)S(1)} %get-tuple-element.67), channel_id=1, source_target_pairs={{0,1},{1,0},{2,3},{3,2},{4,5},{5,4},{6,7},{7,6},{8,15},{9,10},{10,... | collective-permute-start | bytes 405512 | tf_op jit(solution)/shard_map/ppermute | solution.py:26
  189.0 3.2 %collective-permute-start.26 = (bf16[528,256]{1,0:T(8,128)(2,1)S(1)}, bf16[528,256]{1,0:T(8,128)(2,1)S(1)}, u32[]{:S(2)}, u32[]{:S(2)}) collective-permute-start(bf16[528,256]{1,0:T(8,128)(2,1)S(1)} %pad_maximum_fusion.6), channel_id=1, source_target_pairs={{0,7},{1,2},{2,1},{3,4},{4,3},{5,6},{6,5},{7,0},{8,9},{9,8},{10,11... | collective-permute-start | bytes 811016 | tf_op jit(solution)/shard_map/ppermute | solution.py:26
  192.2 1.0 collective-permute-done.9
  193.3 4.5 %collective-permute-start.10 = (bf16[528,256]{1,0:T(8,128)(2,1)S(1)}, bf16[528,256]{1,0:T(8,128)(2,1)S(1)}, u32[]{:S(2)}, u32[]{:S(2)}) collective-permute-start(bf16[528,256]{1,0:T(8,128)(2,1)S(1)} %pad_maximum_fusion.2), channel_id=1, source_target_pairs={{0,7},{1,2},{2,1},{3,4},{4,3},{5,6},{6,5},{7,0},{8,9},{9,8},{10,11... | collective-permute-start | bytes 811016 | tf_op jit(solution)/shard_map/ppermute | solution.py:26
  199.3 2.1 collective-permute-start.27
  202.9 2.9 %collective-permute-done.10 = bf16[528,256]{1,0:T(8,128)(2,1)S(1)} collective-permute-done((bf16[528,256]{1,0:T(8,128)(2,1)S(1)}, bf16[528,256]{1,0:T(8,128)(2,1)S(1)}, u32[]{:S(2)}, u32[]{:S(2)}) %collective-permute-start.10) | collective-permute-done | bytes 270368 | tf_op jit(solution)/shard_map/ppermute | solution.py:26
  205.8 1.9 collective-permute-start.11
  209.2 3.7 %collective-permute-start.28 = (bf16[528,256]{1,0:T(8,128)(2,1)S(1)}, bf16[528,256]{1,0:T(8,128)(2,1)S(1)}, u32[]{:S(2)}, u32[]{:S(2)}) collective-permute-start(bf16[528,256]{1,0:T(8,128)(2,1)S(1)} %collective-permute-done.27), channel_id=1, source_target_pairs={{0,7},{1,2},{2,1},{3,4},{4,3},{5,6},{6,5},{7,0},{8,9},{9,8},{10,11... | collective-permute-start | bytes 811016 | tf_op jit(solution)/shard_map/ppermute | solution.py:26
  214.4 2.2 collective-permute-done.11
  216.6 1.9 collective-permute-start.12
  221.5 2.7 collective-permute-start.29
  224.2 3.4 %collective-permute-done.12 = bf16[528,256]{1,0:T(8,128)(2,1)S(1)} collective-permute-done((bf16[528,256]{1,0:T(8,128)(2,1)S(1)}, bf16[528,256]{1,0:T(8,128)(2,1)S(1)}, u32[]{:S(2)}, u32[]{:S(2)}) %collective-permute-start.12) | collective-permute-done | bytes 270368 | tf_op jit(solution)/shard_map/ppermute | solution.py:26
  229.1 2.0 collective-permute-start.13
  231.3 3.7 %collective-permute-start.30 = (bf16[528,256]{1,0:T(8,128)(2,1)S(1)}, bf16[528,256]{1,0:T(8,128)(2,1)S(1)}, u32[]{:S(2)}, u32[]{:S(2)}) collective-permute-start(bf16[528,256]{1,0:T(8,128)(2,1)S(1)} %pad_maximum_fusion.7), channel_id=1, source_target_pairs={{0,7},{1,2},{2,1},{3,4},{4,3},{5,6},{6,5},{7,0},{8,9},{9,8},{10,11... | collective-permute-start | bytes 811016 | tf_op jit(solution)/shard_map/ppermute | solution.py:26
  235.3 1.2 collective-permute-done.13
  236.5 2.5 collective-permute-start.14
  239.0 4.3 %collective-permute-done.30 = bf16[528,256]{1,0:T(8,128)(2,1)S(1)} collective-permute-done((bf16[528,256]{1,0:T(8,128)(2,1)S(1)}, bf16[528,256]{1,0:T(8,128)(2,1)S(1)}, u32[]{:S(2)}, u32[]{:S(2)}) %collective-permute-start.30) | collective-permute-done | bytes 270368 | tf_op jit(solution)/shard_map/ppermute | solution.py:26
  243.3 1.9 collective-permute-start.31
  245.7 2.4 collective-permute-done.14
  248.1 1.9 collective-permute-start.15
  250.9 0.9 collective-permute-done.31
  251.7 4.8 %collective-permute-start.32 = (bf16[528,256]{1,0:T(8,128)(2,1)S(1)}, bf16[528,256]{1,0:T(8,128)(2,1)S(1)}, u32[]{:S(2)}, u32[]{:S(2)}) collective-permute-start(bf16[528,256]{1,0:T(8,128)(2,1)S(1)} %collective-permute-done.31), channel_id=1, source_target_pairs={{0,7},{1,2},{2,1},{3,4},{4,3},{5,6},{6,5},{7,0},{8,9},{9,8},{10,11... | collective-permute-start | bytes 811016 | tf_op jit(solution)/shard_map/ppermute | solution.py:26
  257.0 0.5 collective-permute-done.15
  257.5 4.2 %collective-permute-start.16 = (bf16[528,256]{1,0:T(8,128)(2,1)S(1)}, bf16[528,256]{1,0:T(8,128)(2,1)S(1)}, u32[]{:S(2)}, u32[]{:S(2)}) collective-permute-start(bf16[528,256]{1,0:T(8,128)(2,1)S(1)} %collective-permute-done.15), channel_id=1, source_target_pairs={{0,7},{1,2},{2,1},{3,4},{4,3},{5,6},{6,5},{7,0},{8,9},{9,8},{10,11... | collective-permute-start | bytes 811016 | tf_op jit(solution)/shard_map/ppermute | solution.py:26
  262.7 4.4 %collective-permute-done.16 = bf16[528,256]{1,0:T(8,128)(2,1)S(1)} collective-permute-done((bf16[528,256]{1,0:T(8,128)(2,1)S(1)}, bf16[528,256]{1,0:T(8,128)(2,1)S(1)}, u32[]{:S(2)}, u32[]{:S(2)}) %collective-permute-start.16) | collective-permute-done | bytes 270368 | tf_op jit(solution)/shard_map/ppermute | solution.py:26
  267.6 0.7 pad_maximum_fusion.9
  (177 shorter events, 29.8 us)
Async XLA Ops:
  6.5 116.7 %all-gather.2.cloned.1.call-start = ((), (), s32[]{:S(2)}) async-start(), calls=%async_computation | async-start | bytes 8650752 | tf_op jit(solution)/shard_map/all_gather | solution.py:72
  9.2 13.0 %collective-permute-start.17 = (bf16[264,256]{1,0:T(8,128)(2,1)S(1)}, bf16[264,256]{1,0:T(8,128)(2,1)S(1)}, u32[]{:S(2)}, u32[]{:S(2)}) collective-permute-start(bf16[264,256]{1,0:T(8,128)(2,1)S(1)} %slice.420), channel_id=1, source_target_pairs={{0,1},{1,0},{2,3},{3,2},{4,5},{5,4},{6,7},{7,6},{8,15},{9,10},{10,... | collective-permute-start | bytes 405512 | tf_op jit(solution)/shard_map/ppermute | solution.py:26
  13.5 5.6 %collective-permute-start = (bf16[8,256]{1,0:T(8,128)(2,1)S(1)}, bf16[8,256]{1,0:T(8,128)(2,1)S(1)}, u32[]{:S(2)}, u32[]{:S(2)}) collective-permute-start(bf16[8,256]{1,0:T(8,128)(2,1)S(1)} %slice.166), channel_id=1, source_target_pairs={{0,8},{8,16},{16,24},{24,32},{32,40},{40,48},{48,56},{56,64},{64,7... | collective-permute-start | bytes 12296 | tf_op jit(solution)/shard_map/ppermute | solution.py:16
  20.2 6.9 %collective-permute-start.1 = (bf16[264,256]{1,0:T(8,128)(2,1)S(1)}, bf16[264,256]{1,0:T(8,128)(2,1)S(1)}, u32[]{:S(2)}, u32[]{:S(2)}) collective-permute-start(bf16[264,256]{1,0:T(8,128)(2,1)S(1)} %get-tuple-element.32), channel_id=1, source_target_pairs={{0,1},{1,0},{2,3},{3,2},{4,5},{5,4},{6,7},{7,6},{8,15},{9,10},{10,... | collective-permute-start | bytes 405512 | tf_op jit(solution)/shard_map/ppermute | solution.py:26
  22.2 11.0 %collective-permute-start.18 = (bf16[528,256]{1,0:T(8,128)(2,1)S(1)}, bf16[528,256]{1,0:T(8,128)(2,1)S(1)}, u32[]{:S(2)}, u32[]{:S(2)}) collective-permute-start(bf16[528,256]{1,0:T(8,128)(2,1)S(1)} %pad_maximum_fusion.4), channel_id=1, source_target_pairs={{0,7},{1,2},{2,1},{3,4},{4,3},{5,6},{6,5},{7,0},{8,9},{9,8},{10,11... | collective-permute-start | bytes 811016 | tf_op jit(solution)/shard_map/ppermute | solution.py:26
  27.2 9.6 %collective-permute-start.2 = (bf16[528,256]{1,0:T(8,128)(2,1)S(1)}, bf16[528,256]{1,0:T(8,128)(2,1)S(1)}, u32[]{:S(2)}, u32[]{:S(2)}) collective-permute-start(bf16[528,256]{1,0:T(8,128)(2,1)S(1)} %pad_maximum_fusion), channel_id=1, source_target_pairs={{0,7},{1,2},{2,1},{3,4},{4,3},{5,6},{6,5},{7,0},{8,9},{9,8},{10,11... | collective-permute-start | bytes 811016 | tf_op jit(solution)/shard_map/ppermute | solution.py:26
  33.2 9.0 %collective-permute-start.19 = (bf16[528,256]{1,0:T(8,128)(2,1)S(1)}, bf16[528,256]{1,0:T(8,128)(2,1)S(1)}, u32[]{:S(2)}, u32[]{:S(2)}) collective-permute-start(bf16[528,256]{1,0:T(8,128)(2,1)S(1)} %collective-permute-done.18), channel_id=1, source_target_pairs={{0,1},{1,0},{2,3},{3,2},{4,5},{5,4},{6,7},{7,6},{8,15},{9,10},{10,... | collective-permute-start | bytes 811016 | tf_op jit(solution)/shard_map/ppermute | solution.py:26
  36.8 10.7 %collective-permute-start.3 = (bf16[528,256]{1,0:T(8,128)(2,1)S(1)}, bf16[528,256]{1,0:T(8,128)(2,1)S(1)}, u32[]{:S(2)}, u32[]{:S(2)}) collective-permute-start(bf16[528,256]{1,0:T(8,128)(2,1)S(1)} %collective-permute-done.2), channel_id=1, source_target_pairs={{0,1},{1,0},{2,3},{3,2},{4,5},{5,4},{6,7},{7,6},{8,15},{9,10},{10,... | collective-permute-start | bytes 811016 | tf_op jit(solution)/shard_map/ppermute | solution.py:26
  42.2 9.7 %collective-permute-start.20 = (bf16[528,256]{1,0:T(8,128)(2,1)S(1)}, bf16[528,256]{1,0:T(8,128)(2,1)S(1)}, u32[]{:S(2)}, u32[]{:S(2)}) collective-permute-start(bf16[528,256]{1,0:T(8,128)(2,1)S(1)} %collective-permute-done.19), channel_id=1, source_target_pairs={{0,7},{1,2},{2,1},{3,4},{4,3},{5,6},{6,5},{7,0},{8,9},{9,8},{10,11... | collective-permute-start | bytes 811016 | tf_op jit(solution)/shard_map/ppermute | solution.py:26
  47.5 9.6 %collective-permute-start.4 = (bf16[528,256]{1,0:T(8,128)(2,1)S(1)}, bf16[528,256]{1,0:T(8,128)(2,1)S(1)}, u32[]{:S(2)}, u32[]{:S(2)}) collective-permute-start(bf16[528,256]{1,0:T(8,128)(2,1)S(1)} %collective-permute-done.3), channel_id=1, source_target_pairs={{0,7},{1,2},{2,1},{3,4},{4,3},{5,6},{6,5},{7,0},{8,9},{9,8},{10,11... | collective-permute-start | bytes 811016 | tf_op jit(solution)/shard_map/ppermute | solution.py:26
  57.3 69.6 %copy-start = (bf16[512,256]{1,0:T(8,128)(2,1)S(1)}, bf16[512,256]{1,0:T(8,128)(2,1)}, u32[]{:S(2)}) copy-start(bf16[512,256]{1,0:T(8,128)(2,1)} %param.7) | copy-start | bytes 786436
  132.6 19.0 %collective-permute-start.21 = (bf16[264,256]{1,0:T(8,128)(2,1)S(1)}, bf16[264,256]{1,0:T(8,128)(2,1)S(1)}, u32[]{:S(2)}, u32[]{:S(2)}) collective-permute-start(bf16[264,256]{1,0:T(8,128)(2,1)S(1)} %fusion.45), channel_id=1, source_target_pairs={{0,1},{1,0},{2,3},{3,2},{4,5},{5,4},{6,7},{7,6},{8,15},{9,10},{10,... | collective-permute-start | bytes 405512 | tf_op jit(solution)/shard_map/ppermute | solution.py:26
  140.1 6.9 %collective-permute-start.5 = (bf16[264,256]{1,0:T(8,128)(2,1)S(1)}, bf16[264,256]{1,0:T(8,128)(2,1)S(1)}, u32[]{:S(2)}, u32[]{:S(2)}) collective-permute-start(bf16[264,256]{1,0:T(8,128)(2,1)S(1)} %fusion.26), channel_id=1, source_target_pairs={{0,1},{1,0},{2,3},{3,2},{4,5},{5,4},{6,7},{7,6},{8,15},{9,10},{10,... | collective-permute-start | bytes 405512 | tf_op jit(solution)/shard_map/ppermute | solution.py:26
  147.0 9.6 %collective-permute-start.6 = (bf16[528,256]{1,0:T(8,128)(2,1)S(1)}, bf16[528,256]{1,0:T(8,128)(2,1)S(1)}, u32[]{:S(2)}, u32[]{:S(2)}) collective-permute-start(bf16[528,256]{1,0:T(8,128)(2,1)S(1)} %pad_maximum_fusion.1), channel_id=1, source_target_pairs={{0,7},{1,2},{2,1},{3,4},{4,3},{5,6},{6,5},{7,0},{8,9},{9,8},{10,11... | collective-permute-start | bytes 811016 | tf_op jit(solution)/shard_map/ppermute | solution.py:26
  151.6 9.6 %collective-permute-start.22 = (bf16[528,256]{1,0:T(8,128)(2,1)S(1)}, bf16[528,256]{1,0:T(8,128)(2,1)S(1)}, u32[]{:S(2)}, u32[]{:S(2)}) collective-permute-start(bf16[528,256]{1,0:T(8,128)(2,1)S(1)} %pad_maximum_fusion.5), channel_id=1, source_target_pairs={{0,7},{1,2},{2,1},{3,4},{4,3},{5,6},{6,5},{7,0},{8,9},{9,8},{10,11... | collective-permute-start | bytes 811016 | tf_op jit(solution)/shard_map/ppermute | solution.py:26
  161.2 8.4 %collective-permute-start.23 = (bf16[528,256]{1,0:T(8,128)(2,1)S(1)}, bf16[528,256]{1,0:T(8,128)(2,1)S(1)}, u32[]{:S(2)}, u32[]{:S(2)}) collective-permute-start(bf16[528,256]{1,0:T(8,128)(2,1)S(1)} %collective-permute-done.22), channel_id=1, source_target_pairs={{0,1},{1,0},{2,3},{3,2},{4,5},{5,4},{6,7},{7,6},{8,15},{9,10},{10,... | collective-permute-start | bytes 811016 | tf_op jit(solution)/shard_map/ppermute | solution.py:26
  163.6 9.6 %collective-permute-start.7 = (bf16[528,256]{1,0:T(8,128)(2,1)S(1)}, bf16[528,256]{1,0:T(8,128)(2,1)S(1)}, u32[]{:S(2)}, u32[]{:S(2)}) collective-permute-start(bf16[528,256]{1,0:T(8,128)(2,1)S(1)} %collective-permute-done.6), channel_id=1, source_target_pairs={{0,1},{1,0},{2,3},{3,2},{4,5},{5,4},{6,7},{7,6},{8,15},{9,10},{10,... | collective-permute-start | bytes 811016 | tf_op jit(solution)/shard_map/ppermute | solution.py:26
  169.6 9.6 %collective-permute-start.24 = (bf16[528,256]{1,0:T(8,128)(2,1)S(1)}, bf16[528,256]{1,0:T(8,128)(2,1)S(1)}, u32[]{:S(2)}, u32[]{:S(2)}) collective-permute-start(bf16[528,256]{1,0:T(8,128)(2,1)S(1)} %collective-permute-done.23), channel_id=1, source_target_pairs={{0,7},{1,2},{2,1},{3,4},{4,3},{5,6},{6,5},{7,0},{8,9},{9,8},{10,11... | collective-permute-start | bytes 811016 | tf_op jit(solution)/shard_map/ppermute | solution.py:26
  173.2 10.9 %collective-permute-start.8 = (bf16[528,256]{1,0:T(8,128)(2,1)S(1)}, bf16[528,256]{1,0:T(8,128)(2,1)S(1)}, u32[]{:S(2)}, u32[]{:S(2)}) collective-permute-start(bf16[528,256]{1,0:T(8,128)(2,1)S(1)} %collective-permute-done.7), channel_id=1, source_target_pairs={{0,7},{1,2},{2,1},{3,4},{4,3},{5,6},{6,5},{7,0},{8,9},{9,8},{10,11... | collective-permute-start | bytes 811016 | tf_op jit(solution)/shard_map/ppermute | solution.py:26
  179.7 9.3 %collective-permute-start.25 = (bf16[264,256]{1,0:T(8,128)(2,1)S(1)}, bf16[264,256]{1,0:T(8,128)(2,1)S(1)}, u32[]{:S(2)}, u32[]{:S(2)}) collective-permute-start(bf16[264,256]{1,0:T(8,128)(2,1)S(1)} %get-tuple-element.65), channel_id=1, source_target_pairs={{0,1},{1,0},{2,3},{3,2},{4,5},{5,4},{6,7},{7,6},{8,15},{9,10},{10,... | collective-permute-start | bytes 405512 | tf_op jit(solution)/shard_map/ppermute | solution.py:26
  184.9 8.4 %collective-permute-start.9 = (bf16[264,256]{1,0:T(8,128)(2,1)S(1)}, bf16[264,256]{1,0:T(8,128)(2,1)S(1)}, u32[]{:S(2)}, u32[]{:S(2)}) collective-permute-start(bf16[264,256]{1,0:T(8,128)(2,1)S(1)} %get-tuple-element.67), channel_id=1, source_target_pairs={{0,1},{1,0},{2,3},{3,2},{4,5},{5,4},{6,7},{7,6},{8,15},{9,10},{10,... | collective-permute-start | bytes 405512 | tf_op jit(solution)/shard_map/ppermute | solution.py:26
  189.0 10.3 %collective-permute-start.26 = (bf16[528,256]{1,0:T(8,128)(2,1)S(1)}, bf16[528,256]{1,0:T(8,128)(2,1)S(1)}, u32[]{:S(2)}, u32[]{:S(2)}) collective-permute-start(bf16[528,256]{1,0:T(8,128)(2,1)S(1)} %pad_maximum_fusion.6), channel_id=1, source_target_pairs={{0,7},{1,2},{2,1},{3,4},{4,3},{5,6},{6,5},{7,0},{8,9},{9,8},{10,11... | collective-permute-start | bytes 811016 | tf_op jit(solution)/shard_map/ppermute | solution.py:26
  193.3 12.5 %collective-permute-start.10 = (bf16[528,256]{1,0:T(8,128)(2,1)S(1)}, bf16[528,256]{1,0:T(8,128)(2,1)S(1)}, u32[]{:S(2)}, u32[]{:S(2)}) collective-permute-start(bf16[528,256]{1,0:T(8,128)(2,1)S(1)} %pad_maximum_fusion.2), channel_id=1, source_target_pairs={{0,7},{1,2},{2,1},{3,4},{4,3},{5,6},{6,5},{7,0},{8,9},{9,8},{10,11... | collective-permute-start | bytes 811016 | tf_op jit(solution)/shard_map/ppermute | solution.py:26
  199.3 9.9 %collective-permute-start.27 = (bf16[528,256]{1,0:T(8,128)(2,1)S(1)}, bf16[528,256]{1,0:T(8,128)(2,1)S(1)}, u32[]{:S(2)}, u32[]{:S(2)}) collective-permute-start(bf16[528,256]{1,0:T(8,128)(2,1)S(1)} %collective-permute-done.26), channel_id=1, source_target_pairs={{0,1},{1,0},{2,3},{3,2},{4,5},{5,4},{6,7},{7,6},{8,15},{9,10},{10,... | collective-permute-start | bytes 811016 | tf_op jit(solution)/shard_map/ppermute | solution.py:26
  205.8 10.8 %collective-permute-start.11 = (bf16[528,256]{1,0:T(8,128)(2,1)S(1)}, bf16[528,256]{1,0:T(8,128)(2,1)S(1)}, u32[]{:S(2)}, u32[]{:S(2)}) collective-permute-start(bf16[528,256]{1,0:T(8,128)(2,1)S(1)} %collective-permute-done.10), channel_id=1, source_target_pairs={{0,1},{1,0},{2,3},{3,2},{4,5},{5,4},{6,7},{7,6},{8,15},{9,10},{10,... | collective-permute-start | bytes 811016 | tf_op jit(solution)/shard_map/ppermute | solution.py:26
  209.2 10.8 %collective-permute-start.28 = (bf16[528,256]{1,0:T(8,128)(2,1)S(1)}, bf16[528,256]{1,0:T(8,128)(2,1)S(1)}, u32[]{:S(2)}, u32[]{:S(2)}) collective-permute-start(bf16[528,256]{1,0:T(8,128)(2,1)S(1)} %collective-permute-done.27), channel_id=1, source_target_pairs={{0,7},{1,2},{2,1},{3,4},{4,3},{5,6},{6,5},{7,0},{8,9},{9,8},{10,11... | collective-permute-start | bytes 811016 | tf_op jit(solution)/shard_map/ppermute | solution.py:26
  216.6 11.0 %collective-permute-start.12 = (bf16[528,256]{1,0:T(8,128)(2,1)S(1)}, bf16[528,256]{1,0:T(8,128)(2,1)S(1)}, u32[]{:S(2)}, u32[]{:S(2)}) collective-permute-start(bf16[528,256]{1,0:T(8,128)(2,1)S(1)} %collective-permute-done.11), channel_id=1, source_target_pairs={{0,7},{1,2},{2,1},{3,4},{4,3},{5,6},{6,5},{7,0},{8,9},{9,8},{10,11... | collective-permute-start | bytes 811016 | tf_op jit(solution)/shard_map/ppermute | solution.py:26
  221.5 9.8 %collective-permute-start.29 = (bf16[264,256]{1,0:T(8,128)(2,1)S(1)}, bf16[264,256]{1,0:T(8,128)(2,1)S(1)}, u32[]{:S(2)}, u32[]{:S(2)}) collective-permute-start(bf16[264,256]{1,0:T(8,128)(2,1)S(1)} %fusion.55), channel_id=1, source_target_pairs={{0,1},{1,0},{2,3},{3,2},{4,5},{5,4},{6,7},{7,6},{8,15},{9,10},{10,... | collective-permute-start | bytes 405512 | tf_op jit(solution)/shard_map/ppermute | solution.py:26
  229.1 7.3 %collective-permute-start.13 = (bf16[264,256]{1,0:T(8,128)(2,1)S(1)}, bf16[264,256]{1,0:T(8,128)(2,1)S(1)}, u32[]{:S(2)}, u32[]{:S(2)}) collective-permute-start(bf16[264,256]{1,0:T(8,128)(2,1)S(1)} %fusion.36), channel_id=1, source_target_pairs={{0,1},{1,0},{2,3},{3,2},{4,5},{5,4},{6,7},{7,6},{8,15},{9,10},{10,... | collective-permute-start | bytes 405512 | tf_op jit(solution)/shard_map/ppermute | solution.py:26
  231.3 12.0 %collective-permute-start.30 = (bf16[528,256]{1,0:T(8,128)(2,1)S(1)}, bf16[528,256]{1,0:T(8,128)(2,1)S(1)}, u32[]{:S(2)}, u32[]{:S(2)}) collective-permute-start(bf16[528,256]{1,0:T(8,128)(2,1)S(1)} %pad_maximum_fusion.7), channel_id=1, source_target_pairs={{0,7},{1,2},{2,1},{3,4},{4,3},{5,6},{6,5},{7,0},{8,9},{9,8},{10,11... | collective-permute-start | bytes 811016 | tf_op jit(solution)/shard_map/ppermute | solution.py:26
  236.5 11.6 %collective-permute-start.14 = (bf16[528,256]{1,0:T(8,128)(2,1)S(1)}, bf16[528,256]{1,0:T(8,128)(2,1)S(1)}, u32[]{:S(2)}, u32[]{:S(2)}) collective-permute-start(bf16[528,256]{1,0:T(8,128)(2,1)S(1)} %pad_maximum_fusion.3), channel_id=1, source_target_pairs={{0,7},{1,2},{2,1},{3,4},{4,3},{5,6},{6,5},{7,0},{8,9},{9,8},{10,11... | collective-permute-start | bytes 811016 | tf_op jit(solution)/shard_map/ppermute | solution.py:26
  243.3 8.4 %collective-permute-start.31 = (bf16[528,256]{1,0:T(8,128)(2,1)S(1)}, bf16[528,256]{1,0:T(8,128)(2,1)S(1)}, u32[]{:S(2)}, u32[]{:S(2)}) collective-permute-start(bf16[528,256]{1,0:T(8,128)(2,1)S(1)} %collective-permute-done.30), channel_id=1, source_target_pairs={{0,1},{1,0},{2,3},{3,2},{4,5},{5,4},{6,7},{7,6},{8,15},{9,10},{10,... | collective-permute-start | bytes 811016 | tf_op jit(solution)/shard_map/ppermute | solution.py:26
  248.1 9.4 %collective-permute-start.15 = (bf16[528,256]{1,0:T(8,128)(2,1)S(1)}, bf16[528,256]{1,0:T(8,128)(2,1)S(1)}, u32[]{:S(2)}, u32[]{:S(2)}) collective-permute-start(bf16[528,256]{1,0:T(8,128)(2,1)S(1)} %collective-permute-done.14), channel_id=1, source_target_pairs={{0,1},{1,0},{2,3},{3,2},{4,5},{5,4},{6,7},{7,6},{8,15},{9,10},{10,... | collective-permute-start | bytes 811016 | tf_op jit(solution)/shard_map/ppermute | solution.py:26
  251.7 10.4 %collective-permute-start.32 = (bf16[528,256]{1,0:T(8,128)(2,1)S(1)}, bf16[528,256]{1,0:T(8,128)(2,1)S(1)}, u32[]{:S(2)}, u32[]{:S(2)}) collective-permute-start(bf16[528,256]{1,0:T(8,128)(2,1)S(1)} %collective-permute-done.31), channel_id=1, source_target_pairs={{0,7},{1,2},{2,1},{3,4},{4,3},{5,6},{6,5},{7,0},{8,9},{9,8},{10,11... | collective-permute-start | bytes 811016 | tf_op jit(solution)/shard_map/ppermute | solution.py:26
  257.5 9.6 %collective-permute-start.16 = (bf16[528,256]{1,0:T(8,128)(2,1)S(1)}, bf16[528,256]{1,0:T(8,128)(2,1)S(1)}, u32[]{:S(2)}, u32[]{:S(2)}) collective-permute-start(bf16[528,256]{1,0:T(8,128)(2,1)S(1)} %collective-permute-done.15), channel_id=1, source_target_pairs={{0,7},{1,2},{2,1},{3,4},{4,3},{5,6},{6,5},{7,0},{8,9},{9,8},{10,11... | collective-permute-start | bytes 811016 | tf_op jit(solution)/shard_map/ppermute | solution.py:26
Sparse Core Ops, SparseCore 0:
  9.5 113.7 all-gather.1

commit v3 on v2

v3 whole, which is shorter than its diff:
```python
import jax
import jax.numpy as jnp
from jax import lax
from jax.sharding import PartitionSpec as P

EPS = 1e-06
TILE_ROWS = 8
CHUNKS = 2
F32 = jnp.float32
BF16 = jnp.bfloat16


def passed_along(x, axis, by):
    devices = lax.axis_size(axis)
    pairs = [(i, i + by) for i in range(devices) if 0 <= i + by < devices]
    return lax.ppermute(x, axis, pairs)


def turned(x, axis, by):
    devices = lax.axis_size(axis)
    return lax.ppermute(x, axis, [(i, (i + by) % devices) for i in range(devices)])


def whole_rows(block, axis):
    devices = lax.axis_size(axis)
    arrived = {0: block}
    up = down = block
    for step in range(1, (devices - 1) // 2 + 1):
        up, down = turned(up, axis, 1), turned(down, axis, -1)
        arrived[-step], arrived[step] = up, down
    if devices % 2 == 0:
        later, up = lax.optimization_barrier((block, up))
        arrived[-step] = up
        arrived[devices // 2] = turned(later, axis, devices // 2)
    offsets = sorted(arrived)
    twice = jnp.concatenate([arrived[k] for k in offsets] * 2, axis=1)
    width = block.shape[1]
    first = (lax.axis_index(axis) + offsets[0] + devices) % devices
    return lax.dynamic_slice_in_dim(twice, (devices - first) % devices * width, devices * width, axis=1)


def side_by_side(shard, axis):
    devices = lax.axis_size(axis)
    copies = jnp.broadcast_to(shard, (devices, *shard.shape))
    pieces = lax.all_to_all(copies, axis, split_axis=0, concat_axis=0, tiled=True)
    return jnp.concatenate([pieces[i] for i in range(devices)], axis=1)


def summed(x, axis):
    devices = lax.axis_size(axis)
    count = -(-x.shape[0] // 128) * 128
    copies = jnp.broadcast_to(jnp.pad(x, (0, count - x.shape[0])).reshape(-1, 128), (devices, count // 128, 128))
    return jnp.sum(lax.all_to_all(copies, axis, split_axis=0, concat_axis=0, tiled=True), axis=0).reshape(-1)[: x.shape[0]]


def swapped(x, step):
    lines, devices = lax.axis_size("sp"), lax.axis_size("tp")
    pairs = []
    for s in range(lines):
        for i in range(devices):
            to = i + 1 if i % 2 == (step + s) % 2 else i - 1
            pairs.append((s * devices + i, s * devices + to % devices))
    return lax.ppermute(x, ("sp", "tp"), pairs)


def arriving(block):
    devices = lax.axis_size("tp")
    me, line = lax.axis_index("tp"), lax.axis_index("sp")
    side = jnp.where(me % 2 == line % 2, 1, -1)
    rows = block.shape[0]

    def owner(k):
        return (me + k * side + devices) % devices

    pair = jnp.concatenate([block, swapped(block, 0)], axis=0)
    blocks = [(owner(0), pair[:rows]), (owner(1), pair[rows:])]
    for step in range(1, devices // 2):
        pair = swapped(pair, step)
        near = -step if step % 2 else step
        far = near - 1 if step % 2 else near + 1
        blocks += [(owner(near), pair[:rows]), (owner(far), pair[rows:])]
    return blocks


def product(a, b):
    return jnp.dot(a, b, preferred_element_type=F32)


def convolve(carried, tap_rows):
    reach = tap_rows.shape[0] - 1
    count = carried.shape[0]
    padded = jnp.concatenate([jnp.zeros((reach, carried.shape[1]), F32), carried], axis=0)
    result = jnp.zeros_like(carried)
    for tap in range(reach + 1):
        result = result + tap_rows[tap].astype(F32) * padded[tap : tap + count]
    return result


def gated(projected, tap_rows):
    gate, inner, values = (p.astype(BF16).astype(F32) for p in projected)
    return (gate * convolve(inner * values, tap_rows)).astype(BF16)


def factor_of(squares, count):
    return lax.rsqrt(squares / count + EPS)


def shards(tokens, mix_gain, gate_weight, mix_weight, value_weight, out_weight, conv_taps):
    _, _, width = gate_weight.shape
    features = mix_gain.shape[1]
    reach = conv_taps.shape[1] - 1
    fringe = -(-reach * 2 // TILE_ROWS) * TILE_ROWS
    inward = (gate_weight, mix_weight, value_weight)
    mine = jnp.concatenate([*inward, out_weight[:1]], axis=0)
    early = lax.all_gather(mine, "sp", axis=1, tiled=True)

    before = passed_along(tokens[tokens.shape[0] - fringe :], "sp", 1)
    stream = jnp.concatenate([before, tokens], axis=0)
    whole = whole_rows(stream, "tp").astype(F32)
    factor = factor_of(jnp.sum(whole * whole, axis=1, keepdims=True), features)
    normed = (whole * factor * mix_gain[0].astype(F32)).astype(BF16)
    scaled = (whole * mix_gain[1].astype(F32)).astype(BF16)

    shared = side_by_side(out_weight[0], "tp")
    shared, normed, scaled = lax.optimization_barrier((shared, normed, scaled))
    out_rows = (shared.astype(F32) * mix_gain[1].astype(F32)).astype(BF16)
    through = [product(out_rows, early[2 * k + 1]).astype(BF16) for k in range(3)]
    late = lax.all_gather(jnp.stack([*through, out_weight[1]]), "sp", axis=1, tiled=True)

    mixed = gated([product(normed, early[2 * k]) for k in range(3)], conv_taps[0])
    straight = [product(scaled, early[2 * k + 1]) for k in range(3)]
    all_mixed, *straight = lax.optimization_barrier((whole_rows(mixed, "tp"), *straight))
    stream = (stream.astype(F32) + product(all_mixed, early[6])).astype(BF16)
    wide = stream.astype(F32)
    squares = summed(jnp.sum(wide * wide, axis=1), "tp")
    factor = factor_of(squares, features)[:, None]

    mixed = gated([(straight[k] + product(all_mixed, late[k])) * factor for k in range(3)], conv_taps[1])
    results = []
    count = tokens.shape[0] // CHUNKS
    for c in range(CHUNKS):
        part = slice(fringe + c * count, fringe + (c + 1) * count)
        total = stream[part].astype(F32)
        for owner, block in arriving(mixed[part]):
            total = total + product(block, lax.dynamic_slice_in_dim(late[3], owner * width, width, axis=0))
        results.append(total.astype(BF16))
    return jnp.concatenate(results, axis=0)


def solution(mesh):
    return jax.shard_map(
        shards,
        mesh=mesh,
        in_specs=(
            P(("grp", "sp"), "tp"),
            P(),
            P(None, "sp", "tp"),
            P(None, "sp", "tp"),
            P(None, "sp", "tp"),
            P(None, "sp", "tp"),
            P(None, None, "tp"),
        ),
        out_specs=P(("grp", "sp"), "tp"),
        check_vma=False,
    )
```

time: 277 us -> 256 us (0.924)
  starting transfers between devices: 101 us -> 90.9 us
  waiting for transfers between devices: 119 us -> 114 us
  matrix products: 26 us -> 22.2 us
    ppermute x32 -> x8, starting transfers between devices: 97.6 us -> 24.1 us  [swapped(): return lax.ppermute(x, ('sp', 'tp'), pairs)]
    ppermute x0 -> x14, starting transfers between devices: none -> 53.5 us  [turned(): lax.ppermute(x, axis, [(i, (i + by) % devices) for i in range(devices)])]
    ppermute x0 -> x14, waiting for transfers between devices: none -> 49.7 us  [turned(): lax.ppermute(x, axis, [(i, (i + by) % devices) for i in range(devices)])]
    ppermute x32 -> x8, waiting for transfers between devices: 53 us -> 14.7 us  [swapped(): return lax.ppermute(x, ('sp', 'tp'), pairs)]
    all_gather x1 -> x2, waiting for transfers between devices: 65.9 us -> 41 us  [the longest x1 41 us: shards(): early = lax.all_gather(mine, 'sp', axis=1, tiled=True)]
    all_to_all x0 -> x2, starting transfers between devices: none -> 11.4 us  [the longest x1 7.32 us: side_by_side(): lax.all_to_all(copies, axis, split_axis=0, concat_axis=0, tiled=True)]
    all_to_all x0 -> x2, waiting for transfers between devices: none -> 8.03 us  [the longest x1 8.03 us: summed(): lax.all_to_all(copies, axis, split_axis=0, concat_axis=0, tiled=True)]
    slice x3, local copies, waits for them, and re-layouts: 5.42 us -> 0.91 us  [the longest x1 0.82 us: shards(): out_weight[1]]
  transfers between devices with their start and end apart: 34 -> 27, of which waited for: 24 -> 15; matrix products, arithmetic and copies ran while one was open for 10% -> 8% of each run, Pallas kernels for 0% -> 0%
where the time goes in v3:
time: 256 us; the launch traced here: 254 us
  waiting for transfers between devices  114 us (45%)
  starting transfers between devices  90.9 us (36%)
  matrix products  22.2 us (9%)
  between operations  14.5 us (6%)
  other arithmetic  6.99 us (3%)
  local copies, waits for them, and re-layouts  6.18 us (2%)
    ppermute x14, starting transfers between devices, turned(): lax.ppermute(x, axis, [(i, (i + by) % devices) for i in range(devices)])  53.5 us
    ppermute x14, waiting for transfers between devices, turned(): lax.ppermute(x, axis, [(i, (i + by) % devices) for i in range(devices)])  49.7 us
    all_gather x1, waiting for transfers between devices, shards(): early = lax.all_gather(mine, 'sp', axis=1, tiled=True)  41 us
    ppermute x8, starting transfers between devices, swapped(): return lax.ppermute(x, ('sp', 'tp'), pairs)  24.1 us
    dot_general x29, matrix products, product(): return jnp.dot(a, b, preferred_element_type=F32)  22.2 us
    ppermute x8, waiting for transfers between devices, swapped(): return lax.ppermute(x, ('sp', 'tp'), pairs)  14.7 us
    all_to_all x1, waiting for transfers between devices, summed(): lax.all_to_all(copies, axis, split_axis=0, concat_axis=0, tiled=True)  8.03 us
    all_to_all x1, starting transfers between devices, side_by_side(): lax.all_to_all(copies, axis, split_axis=0, concat_axis=0, tiled=True)  7.32 us
  transfers between devices with their start and end apart: 27, of which 15 were waited for; matrix products, arithmetic and copies ran while one was open for 8% of the time, Pallas kernels for 0%

profile of v3, /device:TPU:80, one launch (start us, length us, event | category | flops | bytes accessed | tf_op | source)
XLA Modules:
  0.0 254.3 jit_solution(15328859614142939107)
XLA Ops:
  6.6 0.8 fusion.101
  7.4 1.6 pad_maximum_fusion.3
  9.1 0.7 slice.187
  9.8 1.8 collective-permute-start
  11.6 0.7 broadcast_in_dim.4
  12.3 7.3 %all-to-all-start = ((bf16[8,64,256]{2,1,0:T(8,128)(2,1)}), bf16[8,64,256]{2,1,0:T(8,128)(2,1)S(1)}, u32[]{:S(2)}, u32[]{:S(2)}) async-start(bf16[8,64,256]{2,1,0:T(8,128)(2,1)} %broadcast_in_dim.4), calls=%async_computation | async-start | bytes 524288 | tf_op jit(solution)/shard_map/all_to_all | solution.py:45
  19.7 1.0 constant_dynamic-update-slice_fusion
  20.7 3.9 %collective-permute-start.1 = (bf16[520,256]{1,0:T(8,128)(2,1)S(1)}, bf16[520,256]{1,0:T(8,128)(2,1)S(1)}, u32[]{:S(2)}, u32[]{:S(2)}) collective-permute-start(bf16[520,256]{1,0:T(8,128)(2,1)S(1)} %constant_dynamic-update-slice_fusion), channel_id=1, source_target_pairs={{0,1},{1,2},{2,3},{3,4},{4,5},{5,6},{6,7},{7,0},{8,9},{9,10},{10,1... | collective-permute-start | bytes 798728 | tf_op jit(solution)/shard_map/ppermute | solution.py:21
  24.6 3.3 %collective-permute-start.4 = (bf16[520,256]{1,0:T(8,128)(2,1)S(1)}, bf16[520,256]{1,0:T(8,128)(2,1)S(1)}, u32[]{:S(2)}, u32[]{:S(2)}) collective-permute-start(bf16[520,256]{1,0:T(8,128)(2,1)S(1)} %constant_dynamic-update-slice_fusion), channel_id=1, source_target_pairs={{0,7},{1,0},{2,1},{3,2},{4,3},{5,4},{6,5},{7,6},{8,15},{9,8},{10,9... | collective-permute-start | bytes 798728 | tf_op jit(solution)/shard_map/ppermute | solution.py:21
  27.9 0.8 slice_convert_fusion
  28.7 6.7 %collective-permute-done.1 = bf16[520,256]{1,0:T(8,128)(2,1)S(1)} collective-permute-done((bf16[520,256]{1,0:T(8,128)(2,1)S(1)}, bf16[520,256]{1,0:T(8,128)(2,1)S(1)}, u32[]{:S(2)}, u32[]{:S(2)}) %collective-permute-start.1) | collective-permute-done | bytes 266272 | tf_op jit(solution)/shard_map/ppermute | solution.py:21
  35.4 1.9 collective-permute-start.2
  37.3 5.2 %collective-permute-start.5 = (bf16[520,256]{1,0:T(8,128)(2,1)S(1)}, bf16[520,256]{1,0:T(8,128)(2,1)S(1)}, u32[]{:S(2)}, u32[]{:S(2)}) collective-permute-start(bf16[520,256]{1,0:T(8,128)(2,1)S(1)} %collective-permute-done.4), channel_id=1, source_target_pairs={{0,7},{1,0},{2,1},{3,2},{4,3},{5,4},{6,5},{7,6},{8,15},{9,8},{10,9... | collective-permute-start | bytes 798728 | tf_op jit(solution)/shard_map/ppermute | solution.py:21
  42.6 5.2 %collective-permute-done.2 = bf16[520,256]{1,0:T(8,128)(2,1)S(1)} collective-permute-done((bf16[520,256]{1,0:T(8,128)(2,1)S(1)}, bf16[520,256]{1,0:T(8,128)(2,1)S(1)}, u32[]{:S(2)}, u32[]{:S(2)}) %collective-permute-start.2) | collective-permute-done | bytes 266272 | tf_op jit(solution)/shard_map/ppermute | solution.py:21
  47.7 1.9 collective-permute-start.3
  49.7 5.2 %collective-permute-start.6 = (bf16[520,256]{1,0:T(8,128)(2,1)S(1)}, bf16[520,256]{1,0:T(8,128)(2,1)S(1)}, u32[]{:S(2)}, u32[]{:S(2)}) collective-permute-start(bf16[520,256]{1,0:T(8,128)(2,1)S(1)} %collective-permute-done.5), channel_id=1, source_target_pairs={{0,7},{1,0},{2,1},{3,2},{4,3},{5,4},{6,5},{7,6},{8,15},{9,8},{10,9... | collective-permute-start | bytes 798728 | tf_op jit(solution)/shard_map/ppermute | solution.py:21
  54.9 4.4 %collective-permute-done.3 = bf16[520,256]{1,0:T(8,128)(2,1)S(1)} collective-permute-done((bf16[520,256]{1,0:T(8,128)(2,1)S(1)}, bf16[520,256]{1,0:T(8,128)(2,1)S(1)}, u32[]{:S(2)}, u32[]{:S(2)}) %collective-permute-start.3) | collective-permute-done | bytes 266272 | tf_op jit(solution)/shard_map/ppermute | solution.py:21
  59.4 3.5 %collective-permute-start.7 = (bf16[520,256]{1,0:T(8,128)(2,1)S(1)}, bf16[520,256]{1,0:T(8,128)(2,1)S(1)}, u32[]{:S(2)}, u32[]{:S(2)}) collective-permute-start(bf16[520,256]{1,0:T(8,128)(2,1)S(1)} %constant_dynamic-update-slice_fusion), channel_id=1, source_target_pairs={{0,4},{1,5},{2,6},{3,7},{4,0},{5,1},{6,2},{7,3},{8,12},{9,13},{10,... | collective-permute-start | bytes 798728 | tf_op jit(solution)/shard_map/ppermute | solution.py:21
  63.0 15.0 %collective-permute-done.7 = bf16[520,256]{1,0:T(8,128)(2,1)S(1)} collective-permute-done((bf16[520,256]{1,0:T(8,128)(2,1)S(1)}, bf16[520,256]{1,0:T(8,128)(2,1)S(1)}, u32[]{:S(2)}, u32[]{:S(2)}) %collective-permute-start.7) | collective-permute-done | bytes 266272 | tf_op jit(solution)/shard_map/ppermute | solution.py:21
  78.9 2.1 fusion.3
  81.0 41.0 %all-gather.3.cloned.1.call-done = bf16[7,2048,256]{2,1,0:T(8,128)(2,1)} async-done(((bf16[7,64,256]{2,1,0:T(8,128)(2,1)}), bf16[7,2048,256]{2,1,0:T(8,128)(2,1)}) %all-gather.3.cloned.1.call-update) | async-done | bytes 7340048 | tf_op jit(solution)/shard_map/all_gather | solution.py:115
  122.0 1.5 fusion.22
  123.5 1.5 fusion.21
  125.0 1.5 fusion.20
  126.5 0.7 pad_maximum_fusion.4
  127.3 2.7 %fusion.9 = f32[520,256]{1,0:T(8,128)S(1)} fusion(bf16[520,2048]{1,0:T(8,128)(2,1)} %get-tuple-element.18, bf16[7,2048,256]{2,1,0:T(8,128)(2,1)} %all-gather.3.cloned.1.call-done), kind=kOutput, calls=%fused_computation.15 | convolution fusion | flops 545525760 | bytes 3710976 | tf_op jit(solution)/shard_map/dot_general | solution.py:86
  130.1 2.1 fusion.8
  132.2 2.1 fusion.6
  134.4 3.7 %collective-permute-start.8 = (bf16[520,256]{1,0:T(8,128)(2,1)S(1)}, bf16[520,256]{1,0:T(8,128)(2,1)S(1)}, u32[]{:S(2)}, u32[]{:S(2)}) collective-permute-start(bf16[520,256]{1,0:T(8,128)(2,1)S(1)} %fusion.6), channel_id=1, source_target_pairs={{0,1},{1,2},{2,3},{3,4},{4,5},{5,6},{6,7},{7,0},{8,9},{9,10},{10,1... | collective-permute-start | bytes 798728 | tf_op jit(solution)/shard_map/ppermute | solution.py:21
  138.1 3.4 %collective-permute-start.11 = (bf16[520,256]{1,0:T(8,128)(2,1)S(1)}, bf16[520,256]{1,0:T(8,128)(2,1)S(1)}, u32[]{:S(2)}, u32[]{:S(2)}) collective-permute-start(bf16[520,256]{1,0:T(8,128)(2,1)S(1)} %fusion.6), channel_id=1, source_target_pairs={{0,7},{1,0},{2,1},{3,2},{4,3},{5,4},{6,5},{7,6},{8,15},{9,8},{10,9... | collective-permute-start | bytes 798728 | tf_op jit(solution)/shard_map/ppermute | solution.py:21
  141.5 0.8 fusion.27
  142.3 3.8 %collective-permute-done.8 = bf16[520,256]{1,0:T(8,128)(2,1)S(1)} collective-permute-done((bf16[520,256]{1,0:T(8,128)(2,1)S(1)}, bf16[520,256]{1,0:T(8,128)(2,1)S(1)}, u32[]{:S(2)}, u32[]{:S(2)}) %collective-permute-start.8) | collective-permute-done | bytes 266272 | tf_op jit(solution)/shard_map/ppermute | solution.py:21
  146.1 2.4 collective-permute-start.9
  148.5 0.8 fusion.28
  149.3 4.7 %collective-permute-start.12 = (bf16[520,256]{1,0:T(8,128)(2,1)S(1)}, bf16[520,256]{1,0:T(8,128)(2,1)S(1)}, u32[]{:S(2)}, u32[]{:S(2)}) collective-permute-start(bf16[520,256]{1,0:T(8,128)(2,1)S(1)} %collective-permute-done.11), channel_id=1, source_target_pairs={{0,7},{1,0},{2,1},{3,2},{4,3},{5,4},{6,5},{7,6},{8,15},{9,8},{10,9... | collective-permute-start | bytes 798728 | tf_op jit(solution)/shard_map/ppermute | solution.py:21
  154.0 3.0 %collective-permute-done.9 = bf16[520,256]{1,0:T(8,128)(2,1)S(1)} collective-permute-done((bf16[520,256]{1,0:T(8,128)(2,1)S(1)}, bf16[520,256]{1,0:T(8,128)(2,1)S(1)}, u32[]{:S(2)}, u32[]{:S(2)}) %collective-permute-start.9) | collective-permute-done | bytes 266272 | tf_op jit(solution)/shard_map/ppermute | solution.py:21
  157.0 1.9 collective-permute-start.10
  158.9 1.6 fusion.29
  160.5 5.2 %collective-permute-start.13 = (bf16[520,256]{1,0:T(8,128)(2,1)S(1)}, bf16[520,256]{1,0:T(8,128)(2,1)S(1)}, u32[]{:S(2)}, u32[]{:S(2)}) collective-permute-start(bf16[520,256]{1,0:T(8,128)(2,1)S(1)} %collective-permute-done.12), channel_id=1, source_target_pairs={{0,7},{1,0},{2,1},{3,2},{4,3},{5,4},{6,5},{7,6},{8,15},{9,8},{10,9... | collective-permute-start | bytes 798728 | tf_op jit(solution)/shard_map/ppermute | solution.py:21
  165.7 1.5 collective-permute-done.10
  167.3 7.4 %collective-permute-start.14 = (bf16[520,256]{1,0:T(8,128)(2,1)S(1)}, bf16[520,256]{1,0:T(8,128)(2,1)S(1)}, u32[]{:S(2)}, u32[]{:S(2)}) collective-permute-start(bf16[520,256]{1,0:T(8,128)(2,1)S(1)} %fusion.6), channel_id=1, source_target_pairs={{0,4},{1,5},{2,6},{3,7},{4,0},{5,1},{6,2},{7,3},{8,12},{9,13},{10,... | collective-permute-start | bytes 798728 | tf_op jit(solution)/shard_map/ppermute | solution.py:21
  174.8 10.2 %collective-permute-done.14 = bf16[520,256]{1,0:T(8,128)(2,1)S(1)} collective-permute-done((bf16[520,256]{1,0:T(8,128)(2,1)S(1)}, bf16[520,256]{1,0:T(8,128)(2,1)S(1)}, u32[]{:S(2)}, u32[]{:S(2)}) %collective-permute-start.14) | collective-permute-done | bytes 266272 | tf_op jit(solution)/shard_map/ppermute | solution.py:21
  185.5 0.5 copy-done.6
  186.0 0.8 multiply_reduce_fusion
  186.8 0.6 broadcast_in_dim.5
  187.5 4.1 %all-to-all-start.1 = ((f32[8,5,128]{2,1,0:T(8,128)}), f32[8,5,128]{2,1,0:T(8,128)S(1)}, u32[]{:S(2)}, u32[]{:S(2)}) async-start(f32[8,5,128]{2,1,0:T(8,128)} %broadcast_in_dim.5), calls=%async_computation.1 | async-start | bytes 65536 | tf_op jit(solution)/shard_map/all_to_all | solution.py:53
  191.6 8.0 %all-to-all-done.1 = f32[8,5,128]{2,1,0:T(8,128)S(1)} async-done(((f32[8,5,128]{2,1,0:T(8,128)}), f32[8,5,128]{2,1,0:T(8,128)S(1)}, u32[]{:S(2)}, u32[]{:S(2)}) %all-to-all-start.1) | async-done | bytes 20512 | tf_op jit(solution)/shard_map/all_to_all | solution.py:53
  199.7 2.1 fusion.24
  202.2 0.8 fusion.23
  203.4 0.8 fusion.25
  204.5 3.1 %collective-permute-start.19 = (bf16[256,256]{1,0:T(8,128)(2,1)S(1)}, bf16[256,256]{1,0:T(8,128)(2,1)S(1)}, u32[]{:S(2)}, u32[]{:S(2)}) collective-permute-start(bf16[256,256]{1,0:T(8,128)(2,1)S(1)} %get-tuple-element.32), channel_id=1, source_target_pairs={{0,1},{1,0},{2,3},{3,2},{4,5},{5,4},{6,7},{7,6},{8,15},{9,10},{10,... | collective-permute-start | bytes 393224 | tf_op jit(solution)/shard_map/ppermute | solution.py:63
  207.6 2.8 %collective-permute-start.15 = (bf16[256,256]{1,0:T(8,128)(2,1)S(1)}, bf16[256,256]{1,0:T(8,128)(2,1)S(1)}, u32[]{:S(2)}, u32[]{:S(2)}) collective-permute-start(bf16[256,256]{1,0:T(8,128)(2,1)S(1)} %get-tuple-element.31), channel_id=1, source_target_pairs={{0,1},{1,0},{2,3},{3,2},{4,5},{5,4},{6,7},{7,6},{8,15},{9,10},{10,... | collective-permute-start | bytes 393224 | tf_op jit(solution)/shard_map/ppermute | solution.py:63
  210.7 0.7 collective-permute-done.19
  211.4 4.5 %collective-permute-start.20 = (bf16[512,256]{1,0:T(8,128)(2,1)S(1)}, bf16[512,256]{1,0:T(8,128)(2,1)S(1)}, u32[]{:S(2)}, u32[]{:S(2)}) collective-permute-start(bf16[512,256]{1,0:T(8,128)(2,1)S(1)} %pad_maximum_fusion.1), channel_id=1, source_target_pairs={{0,7},{1,2},{2,1},{3,4},{4,3},{5,6},{6,5},{7,0},{8,9},{9,8},{10,11... | collective-permute-start | bytes 786440 | tf_op jit(solution)/shard_map/ppermute | solution.py:63
  215.9 3.5 %collective-permute-start.16 = (bf16[512,256]{1,0:T(8,128)(2,1)S(1)}, bf16[512,256]{1,0:T(8,128)(2,1)S(1)}, u32[]{:S(2)}, u32[]{:S(2)}) collective-permute-start(bf16[512,256]{1,0:T(8,128)(2,1)S(1)} %pad_maximum_fusion), channel_id=1, source_target_pairs={{0,7},{1,2},{2,1},{3,4},{4,3},{5,6},{6,5},{7,0},{8,9},{9,8},{10,11... | collective-permute-start | bytes 786440 | tf_op jit(solution)/shard_map/ppermute | solution.py:63
  219.6 1.3 collective-permute-done.20
  220.9 1.9 collective-permute-start.21
  223.1 3.3 %collective-permute-done.16 = bf16[512,256]{1,0:T(8,128)(2,1)S(1)} collective-permute-done((bf16[512,256]{1,0:T(8,128)(2,1)S(1)}, bf16[512,256]{1,0:T(8,128)(2,1)S(1)}, u32[]{:S(2)}, u32[]{:S(2)}) %collective-permute-start.16) | collective-permute-done | bytes 262176 | tf_op jit(solution)/shard_map/ppermute | solution.py:63
  226.3 1.9 collective-permute-start.17
  229.3 4.4 %collective-permute-start.22 = (bf16[512,256]{1,0:T(8,128)(2,1)S(1)}, bf16[512,256]{1,0:T(8,128)(2,1)S(1)}, u32[]{:S(2)}, u32[]{:S(2)}) collective-permute-start(bf16[512,256]{1,0:T(8,128)(2,1)S(1)} %collective-permute-done.21), channel_id=1, source_target_pairs={{0,7},{1,2},{2,1},{3,4},{4,3},{5,6},{6,5},{7,0},{8,9},{9,8},{10,11... | collective-permute-start | bytes 786440 | tf_op jit(solution)/shard_map/ppermute | solution.py:63
  233.9 2.8 %collective-permute-done.17 = bf16[512,256]{1,0:T(8,128)(2,1)S(1)} collective-permute-done((bf16[512,256]{1,0:T(8,128)(2,1)S(1)}, bf16[512,256]{1,0:T(8,128)(2,1)S(1)}, u32[]{:S(2)}, u32[]{:S(2)}) %collective-permute-start.17) | collective-permute-done | bytes 262176 | tf_op jit(solution)/shard_map/ppermute | solution.py:63
  236.6 1.9 collective-permute-start.18
  239.4 6.7 %collective-permute-done.18 = bf16[512,256]{1,0:T(8,128)(2,1)S(1)} collective-permute-done((bf16[512,256]{1,0:T(8,128)(2,1)S(1)}, bf16[512,256]{1,0:T(8,128)(2,1)S(1)}, u32[]{:S(2)}, u32[]{:S(2)}) %collective-permute-start.18) | collective-permute-done | bytes 262176 | tf_op jit(solution)/shard_map/ppermute | solution.py:63
  246.7 0.7 pad_maximum_fusion.2
  (106 shorter events, 6.2 us)
Async XLA Ops:
  6.5 52.8 %copy-start = (bf16[512,256]{1,0:T(8,128)(2,1)S(1)}, bf16[512,256]{1,0:T(8,128)(2,1)}, u32[]{:S(2)}) copy-start(bf16[512,256]{1,0:T(8,128)(2,1)} %param.7) | copy-start | bytes 786436
  6.5 115.4 %all-gather.3.cloned.1.call-start = ((), (), s32[]{:S(2)}) async-start(), calls=%async_computation.2 | async-start | bytes 7569408 | tf_op jit(solution)/shard_map/all_gather | solution.py:115
  9.8 10.0 %collective-permute-start = (bf16[8,256]{1,0:T(8,128)(2,1)S(1)}, bf16[8,256]{1,0:T(8,128)(2,1)S(1)}, u32[]{:S(2)}, u32[]{:S(2)}) collective-permute-start(bf16[8,256]{1,0:T(8,128)(2,1)S(1)} %slice.187), channel_id=1, source_target_pairs={{0,8},{8,16},{16,24},{24,32},{32,40},{40,48},{48,56},{56,64},{64,7... | collective-permute-start | bytes 12296 | tf_op jit(solution)/shard_map/ppermute | solution.py:16
  12.3 30.2 %all-to-all-start = ((bf16[8,64,256]{2,1,0:T(8,128)(2,1)}), bf16[8,64,256]{2,1,0:T(8,128)(2,1)S(1)}, u32[]{:S(2)}, u32[]{:S(2)}) async-start(bf16[8,64,256]{2,1,0:T(8,128)(2,1)} %broadcast_in_dim.4), calls=%async_computation | async-start | bytes 524288 | tf_op jit(solution)/shard_map/all_to_all | solution.py:45
  19.6 180.0 %all-gather.5.cloned.1.call-start = ((), (), s32[]{:S(2)}) async-start(), calls=%async_computation.3 | async-start | bytes 4325376 | tf_op jit(solution)/shard_map/all_gather | solution.py:128
  20.7 57.6 %copy-start.5 = (bf16[520,256]{1,0:T(8,128)(2,1)}, bf16[520,256]{1,0:T(8,128)(2,1)S(1)}, u32[]{:S(2)}) copy-start(bf16[520,256]{1,0:T(8,128)(2,1)S(1)} %constant_dynamic-update-slice_fusion) | copy-start | bytes 798724
  20.7 14.6 %collective-permute-start.1 = (bf16[520,256]{1,0:T(8,128)(2,1)S(1)}, bf16[520,256]{1,0:T(8,128)(2,1)S(1)}, u32[]{:S(2)}, u32[]{:S(2)}) collective-permute-start(bf16[520,256]{1,0:T(8,128)(2,1)S(1)} %constant_dynamic-update-slice_fusion), channel_id=1, source_target_pairs={{0,1},{1,2},{2,3},{3,4},{4,5},{5,6},{6,7},{7,0},{8,9},{9,10},{10,1... | collective-permute-start | bytes 798728 | tf_op jit(solution)/shard_map/ppermute | solution.py:21
  24.6 12.7 %collective-permute-start.4 = (bf16[520,256]{1,0:T(8,128)(2,1)S(1)}, bf16[520,256]{1,0:T(8,128)(2,1)S(1)}, u32[]{:S(2)}, u32[]{:S(2)}) collective-permute-start(bf16[520,256]{1,0:T(8,128)(2,1)S(1)} %constant_dynamic-update-slice_fusion), channel_id=1, source_target_pairs={{0,7},{1,0},{2,1},{3,2},{4,3},{5,4},{6,5},{7,6},{8,15},{9,8},{10,9... | collective-permute-start | bytes 798728 | tf_op jit(solution)/shard_map/ppermute | solution.py:21
  35.4 12.4 %collective-permute-start.2 = (bf16[520,256]{1,0:T(8,128)(2,1)S(1)}, bf16[520,256]{1,0:T(8,128)(2,1)S(1)}, u32[]{:S(2)}, u32[]{:S(2)}) collective-permute-start(bf16[520,256]{1,0:T(8,128)(2,1)S(1)} %collective-permute-done.1), channel_id=1, source_target_pairs={{0,1},{1,2},{2,3},{3,4},{4,5},{5,6},{6,7},{7,0},{8,9},{9,10},{10,1... | collective-permute-start | bytes 798728 | tf_op jit(solution)/shard_map/ppermute | solution.py:21
  37.3 12.4 %collective-permute-start.5 = (bf16[520,256]{1,0:T(8,128)(2,1)S(1)}, bf16[520,256]{1,0:T(8,128)(2,1)S(1)}, u32[]{:S(2)}, u32[]{:S(2)}) collective-permute-start(bf16[520,256]{1,0:T(8,128)(2,1)S(1)} %collective-permute-done.4), channel_id=1, source_target_pairs={{0,7},{1,0},{2,1},{3,2},{4,3},{5,4},{6,5},{7,6},{8,15},{9,8},{10,9... | collective-permute-start | bytes 798728 | tf_op jit(solution)/shard_map/ppermute | solution.py:21
  47.7 11.5 %collective-permute-start.3 = (bf16[520,256]{1,0:T(8,128)(2,1)S(1)}, bf16[520,256]{1,0:T(8,128)(2,1)S(1)}, u32[]{:S(2)}, u32[]{:S(2)}) collective-permute-start(bf16[520,256]{1,0:T(8,128)(2,1)S(1)} %collective-permute-done.2), channel_id=1, source_target_pairs={{0,1},{1,2},{2,3},{3,4},{4,5},{5,6},{6,7},{7,0},{8,9},{9,10},{10,1... | collective-permute-start | bytes 798728 | tf_op jit(solution)/shard_map/ppermute | solution.py:21
  49.7 13.3 %collective-permute-start.6 = (bf16[520,256]{1,0:T(8,128)(2,1)S(1)}, bf16[520,256]{1,0:T(8,128)(2,1)S(1)}, u32[]{:S(2)}, u32[]{:S(2)}) collective-permute-start(bf16[520,256]{1,0:T(8,128)(2,1)S(1)} %collective-permute-done.5), channel_id=1, source_target_pairs={{0,7},{1,0},{2,1},{3,2},{4,3},{5,4},{6,5},{7,6},{8,15},{9,8},{10,9... | collective-permute-start | bytes 798728 | tf_op jit(solution)/shard_map/ppermute | solution.py:21
  59.4 18.6 %collective-permute-start.7 = (bf16[520,256]{1,0:T(8,128)(2,1)S(1)}, bf16[520,256]{1,0:T(8,128)(2,1)S(1)}, u32[]{:S(2)}, u32[]{:S(2)}) collective-permute-start(bf16[520,256]{1,0:T(8,128)(2,1)S(1)} %constant_dynamic-update-slice_fusion), channel_id=1, source_target_pairs={{0,4},{1,5},{2,6},{3,7},{4,0},{5,1},{6,2},{7,3},{8,12},{9,13},{10,... | collective-permute-start | bytes 798728 | tf_op jit(solution)/shard_map/ppermute | solution.py:21
  78.8 48.4 %copy-start.4 = (bf16[2,3,256]{2,0,1:T(2,128)(2,1)S(1)}, bf16[2,3,256]{2,0,1:T(2,128)(2,1)}, u32[]{:S(2)}) copy-start(bf16[2,3,256]{2,0,1:T(2,128)(2,1)} %param.13) | copy-start | bytes 9220
  127.3 2.8 %copy-start.1 = (bf16[520,2048]{1,0:T(8,128)(2,1)S(1)}, bf16[520,2048]{1,0:T(8,128)(2,1)}, u32[]{:S(2)}) copy-start(bf16[520,2048]{1,0:T(8,128)(2,1)} %get-tuple-element.18) | copy-start | bytes 6389764
  130.1 11.4 %slice-start = ((s8[7340032]{0:T(1024)(128)(4,1)}), s8[4194304]{0:T(1024)(128)(4,1)S(1)}, s32[]{:S(2)}) async-start(s8[7340032]{0:T(1024)(128)(4,1)} %bitcast.150), calls=%async_computation.4 | async-start | bytes 8388608
  132.2 9.3 %slice-start.1 = ((s8[7340032]{0:T(1024)(128)(4,1)}), s8[3145728]{0:T(1024)(128)(4,1)S(1)}, s32[]{:S(2)}) async-start(s8[7340032]{0:T(1024)(128)(4,1)} %bitcast.150), calls=%async_computation.5 | async-start | bytes 6291456
  134.4 11.7 %collective-permute-start.8 = (bf16[520,256]{1,0:T(8,128)(2,1)S(1)}, bf16[520,256]{1,0:T(8,128)(2,1)S(1)}, u32[]{:S(2)}, u32[]{:S(2)}) collective-permute-start(bf16[520,256]{1,0:T(8,128)(2,1)S(1)} %fusion.6), channel_id=1, source_target_pairs={{0,1},{1,2},{2,3},{3,4},{4,5},{5,6},{6,7},{7,0},{8,9},{9,10},{10,1... | collective-permute-start | bytes 798728 | tf_op jit(solution)/shard_map/ppermute | solution.py:21
  138.1 11.2 %collective-permute-start.11 = (bf16[520,256]{1,0:T(8,128)(2,1)S(1)}, bf16[520,256]{1,0:T(8,128)(2,1)S(1)}, u32[]{:S(2)}, u32[]{:S(2)}) collective-permute-start(bf16[520,256]{1,0:T(8,128)(2,1)S(1)} %fusion.6), channel_id=1, source_target_pairs={{0,7},{1,0},{2,1},{3,2},{4,3},{5,4},{6,5},{7,6},{8,15},{9,8},{10,9... | collective-permute-start | bytes 798728 | tf_op jit(solution)/shard_map/ppermute | solution.py:21
  146.1 10.9 %collective-permute-start.9 = (bf16[520,256]{1,0:T(8,128)(2,1)S(1)}, bf16[520,256]{1,0:T(8,128)(2,1)S(1)}, u32[]{:S(2)}, u32[]{:S(2)}) collective-permute-start(bf16[520,256]{1,0:T(8,128)(2,1)S(1)} %collective-permute-done.8), channel_id=1, source_target_pairs={{0,1},{1,2},{2,3},{3,4},{4,5},{5,6},{6,7},{7,0},{8,9},{9,10},{10,1... | collective-permute-start | bytes 798728 | tf_op jit(solution)/shard_map/ppermute | solution.py:21
  149.3 11.2 %collective-permute-start.12 = (bf16[520,256]{1,0:T(8,128)(2,1)S(1)}, bf16[520,256]{1,0:T(8,128)(2,1)S(1)}, u32[]{:S(2)}, u32[]{:S(2)}) collective-permute-start(bf16[520,256]{1,0:T(8,128)(2,1)S(1)} %collective-permute-done.11), channel_id=1, source_target_pairs={{0,7},{1,0},{2,1},{3,2},{4,3},{5,4},{6,5},{7,6},{8,15},{9,8},{10,9... | collective-permute-start | bytes 798728 | tf_op jit(solution)/shard_map/ppermute | solution.py:21
  157.0 10.1 %collective-permute-start.10 = (bf16[520,256]{1,0:T(8,128)(2,1)S(1)}, bf16[520,256]{1,0:T(8,128)(2,1)S(1)}, u32[]{:S(2)}, u32[]{:S(2)}) collective-permute-start(bf16[520,256]{1,0:T(8,128)(2,1)S(1)} %collective-permute-done.9), channel_id=1, source_target_pairs={{0,1},{1,2},{2,3},{3,4},{4,5},{5,6},{6,7},{7,0},{8,9},{9,10},{10,1... | collective-permute-start | bytes 798728 | tf_op jit(solution)/shard_map/ppermute | solution.py:21
  160.5 14.2 %collective-permute-start.13 = (bf16[520,256]{1,0:T(8,128)(2,1)S(1)}, bf16[520,256]{1,0:T(8,128)(2,1)S(1)}, u32[]{:S(2)}, u32[]{:S(2)}) collective-permute-start(bf16[520,256]{1,0:T(8,128)(2,1)S(1)} %collective-permute-done.12), channel_id=1, source_target_pairs={{0,7},{1,0},{2,1},{3,2},{4,3},{5,4},{6,5},{7,6},{8,15},{9,8},{10,9... | collective-permute-start | bytes 798728 | tf_op jit(solution)/shard_map/ppermute | solution.py:21
  167.3 17.7 %collective-permute-start.14 = (bf16[520,256]{1,0:T(8,128)(2,1)S(1)}, bf16[520,256]{1,0:T(8,128)(2,1)S(1)}, u32[]{:S(2)}, u32[]{:S(2)}) collective-permute-start(bf16[520,256]{1,0:T(8,128)(2,1)S(1)} %fusion.6), channel_id=1, source_target_pairs={{0,4},{1,5},{2,6},{3,7},{4,0},{5,1},{6,2},{7,3},{8,12},{9,13},{10,... | collective-permute-start | bytes 798728 | tf_op jit(solution)/shard_map/ppermute | solution.py:21
  185.0 1.0 copy-start.6
  187.5 12.1 %all-to-all-start.1 = ((f32[8,5,128]{2,1,0:T(8,128)}), f32[8,5,128]{2,1,0:T(8,128)S(1)}, u32[]{:S(2)}, u32[]{:S(2)}) async-start(f32[8,5,128]{2,1,0:T(8,128)} %broadcast_in_dim.5), calls=%async_computation.1 | async-start | bytes 65536 | tf_op jit(solution)/shard_map/all_to_all | solution.py:53
  199.7 2.5 copy-start.3
  202.2 1.0 copy-start.2
  204.5 6.9 %collective-permute-start.19 = (bf16[256,256]{1,0:T(8,128)(2,1)S(1)}, bf16[256,256]{1,0:T(8,128)(2,1)S(1)}, u32[]{:S(2)}, u32[]{:S(2)}) collective-permute-start(bf16[256,256]{1,0:T(8,128)(2,1)S(1)} %get-tuple-element.32), channel_id=1, source_target_pairs={{0,1},{1,0},{2,3},{3,2},{4,5},{5,4},{6,7},{7,6},{8,15},{9,10},{10,... | collective-permute-start | bytes 393224 | tf_op jit(solution)/shard_map/ppermute | solution.py:63
  207.6 8.4 %collective-permute-start.15 = (bf16[256,256]{1,0:T(8,128)(2,1)S(1)}, bf16[256,256]{1,0:T(8,128)(2,1)S(1)}, u32[]{:S(2)}, u32[]{:S(2)}) collective-permute-start(bf16[256,256]{1,0:T(8,128)(2,1)S(1)} %get-tuple-element.31), channel_id=1, source_target_pairs={{0,1},{1,0},{2,3},{3,2},{4,5},{5,4},{6,7},{7,6},{8,15},{9,10},{10,... | collective-permute-start | bytes 393224 | tf_op jit(solution)/shard_map/ppermute | solution.py:63
  211.4 9.5 %collective-permute-start.20 = (bf16[512,256]{1,0:T(8,128)(2,1)S(1)}, bf16[512,256]{1,0:T(8,128)(2,1)S(1)}, u32[]{:S(2)}, u32[]{:S(2)}) collective-permute-start(bf16[512,256]{1,0:T(8,128)(2,1)S(1)} %pad_maximum_fusion.1), channel_id=1, source_target_pairs={{0,7},{1,2},{2,1},{3,4},{4,3},{5,6},{6,5},{7,0},{8,9},{9,8},{10,11... | collective-permute-start | bytes 786440 | tf_op jit(solution)/shard_map/ppermute | solution.py:63
  215.9 10.4 %collective-permute-start.16 = (bf16[512,256]{1,0:T(8,128)(2,1)S(1)}, bf16[512,256]{1,0:T(8,128)(2,1)S(1)}, u32[]{:S(2)}, u32[]{:S(2)}) collective-permute-start(bf16[512,256]{1,0:T(8,128)(2,1)S(1)} %pad_maximum_fusion), channel_id=1, source_target_pairs={{0,7},{1,2},{2,1},{3,4},{4,3},{5,6},{6,5},{7,0},{8,9},{9,8},{10,11... | collective-permute-start | bytes 786440 | tf_op jit(solution)/shard_map/ppermute | solution.py:63
  220.9 8.4 %collective-permute-start.21 = (bf16[512,256]{1,0:T(8,128)(2,1)S(1)}, bf16[512,256]{1,0:T(8,128)(2,1)S(1)}, u32[]{:S(2)}, u32[]{:S(2)}) collective-permute-start(bf16[512,256]{1,0:T(8,128)(2,1)S(1)} %collective-permute-done.20), channel_id=1, source_target_pairs={{0,1},{1,0},{2,3},{3,2},{4,5},{5,4},{6,7},{7,6},{8,15},{9,10},{10,... | collective-permute-start | bytes 786440 | tf_op jit(solution)/shard_map/ppermute | solution.py:63
  226.3 10.3 %collective-permute-start.17 = (bf16[512,256]{1,0:T(8,128)(2,1)S(1)}, bf16[512,256]{1,0:T(8,128)(2,1)S(1)}, u32[]{:S(2)}, u32[]{:S(2)}) collective-permute-start(bf16[512,256]{1,0:T(8,128)(2,1)S(1)} %collective-permute-done.16), channel_id=1, source_target_pairs={{0,1},{1,0},{2,3},{3,2},{4,5},{5,4},{6,7},{7,6},{8,15},{9,10},{10,... | collective-permute-start | bytes 786440 | tf_op jit(solution)/shard_map/ppermute | solution.py:63
  229.3 9.9 %collective-permute-start.22 = (bf16[512,256]{1,0:T(8,128)(2,1)S(1)}, bf16[512,256]{1,0:T(8,128)(2,1)S(1)}, u32[]{:S(2)}, u32[]{:S(2)}) collective-permute-start(bf16[512,256]{1,0:T(8,128)(2,1)S(1)} %collective-permute-done.21), channel_id=1, source_target_pairs={{0,7},{1,2},{2,1},{3,4},{4,3},{5,6},{6,5},{7,0},{8,9},{9,8},{10,11... | collective-permute-start | bytes 786440 | tf_op jit(solution)/shard_map/ppermute | solution.py:63
  236.6 9.5 %collective-permute-start.18 = (bf16[512,256]{1,0:T(8,128)(2,1)S(1)}, bf16[512,256]{1,0:T(8,128)(2,1)S(1)}, u32[]{:S(2)}, u32[]{:S(2)}) collective-permute-start(bf16[512,256]{1,0:T(8,128)(2,1)S(1)} %collective-permute-done.17), channel_id=1, source_target_pairs={{0,7},{1,2},{2,1},{3,4},{4,3},{5,6},{6,5},{7,0},{8,9},{9,8},{10,11... | collective-permute-start | bytes 786440 | tf_op jit(solution)/shard_map/ppermute | solution.py:63
Sparse Core Ops, SparseCore 0:
  9.5 112.4 all-gather.2
  127.4 71.9 all-gather.4

commit v4 on v3

--- a/solution.py
+++ b/solution.py
@@ -1,6 +1,7 @@
 import jax
 import jax.numpy as jnp
 from jax import lax
+from jax.experimental import pallas as pl
 from jax.sharding import PartitionSpec as P
 
 EPS = 1e-06
@@ -86,6 +87,35 @@
     return jnp.dot(a, b, preferred_element_type=F32)
 
 
+def through_kernel(rows, weight, own, out):
+    @pl.when(pl.program_id(0) < 3)
+    def _():
+        out[0] = product(rows[...], weight[0]).astype(out.dtype)
+
+    @pl.when(pl.program_id(0) == 3)
+    def _():
+        out[0] = own[...]
+
+
+def through(rows, weights, own):
+    count, depth = rows.shape
+    width = own.shape[1]
+    return pl.pallas_call(
+        through_kernel,
+        grid=(4,),
+        out_shape=jax.ShapeDtypeStruct((4, count, width), BF16),
+        in_specs=[
+            pl.BlockSpec((count, depth), lambda j: (0, 0)),
+            pl.BlockSpec((1, depth, width), lambda j: (jnp.minimum(2 * j + 1, 5), 0, 0)),
+            pl.BlockSpec((count, width), lambda j: (0, 0)),
+        ],
+        out_specs=pl.BlockSpec((1, count, width), lambda j: (j, 0, 0)),
+        cost_estimate=pl.CostEstimate(
+            flops=6 * count * depth * width, bytes_accessed=6 * depth * width, transcendentals=0
+        ),
+    )(rows, weights, own)
+
+
 def convolve(carried, tap_rows):
     reach = tap_rows.shape[0] - 1
     count = carried.shape[0]
@@ -124,8 +154,7 @@
     shared = side_by_side(out_weight[0], "tp")
     shared, normed, scaled = lax.optimization_barrier((shared, normed, scaled))
     out_rows = (shared.astype(F32) * mix_gain[1].astype(F32)).astype(BF16)
-    through = [product(out_rows, early[2 * k + 1]).astype(BF16) for k in range(3)]
-    late = lax.all_gather(jnp.stack([*through, out_weight[1]]), "sp", axis=1, tiled=True)
+    late = lax.all_gather(through(out_rows, early, out_weight[1]), "sp", axis=1, tiled=True)
 
     mixed = gated([product(normed, early[2 * k]) for k in range(3)], conv_taps[0])
     straight = [product(scaled, early[2 * k + 1]) for k in range(3)]

time: 256 us -> 256 us (level)
  Pallas kernels: 0 us -> 3.94 us
  matrix products: 22.2 us -> 18.5 us
    pallas_call x0 -> x1, Pallas kernels: none -> 3.94 us  [through(): pl.pallas_call(through_kernel, grid=(4,), out_shape=jax.ShapeDtypeStruct(...]
    dot_general x29 -> x26, matrix products: 22.2 us -> 18.5 us  [product(): return jnp.dot(a, b, preferred_element_type=F32)]
  transfers between devices with their start and end apart: 27 -> 27, of which waited for: 15 -> 16; matrix products, arithmetic and copies ran while one was open for 8% -> 9% of each run, Pallas kernels for 0% -> 0%
where the time goes in v4:
time: 256 us; the launch traced here: 255 us
  waiting for transfers between devices  112 us (44%)
  starting transfers between devices  91.3 us (36%)
  matrix products  18.5 us (7%)
  between operations  14.4 us (6%)
  other arithmetic  7.65 us (3%)
  local copies, waits for them, and re-layouts  7.48 us (3%)
  Pallas kernels  3.94 us (2%)
    ppermute x14, starting transfers between devices, turned(): lax.ppermute(x, axis, [(i, (i + by) % devices) for i in range(devices)])  53.4 us
    ppermute x14, waiting for transfers between devices, turned(): lax.ppermute(x, axis, [(i, (i + by) % devices) for i in range(devices)])  48.2 us
    all_gather x1, waiting for transfers between devices, shards(): early = lax.all_gather(mine, 'sp', axis=1, tiled=True)  39.3 us
    ppermute x8, starting transfers between devices, swapped(): return lax.ppermute(x, ('sp', 'tp'), pairs)  24.4 us
    dot_general x26, matrix products, product(): return jnp.dot(a, b, preferred_element_type=F32)  18.5 us
    ppermute x8, waiting for transfers between devices, swapped(): return lax.ppermute(x, ('sp', 'tp'), pairs)  15.2 us
    all_to_all x1, waiting for transfers between devices, summed(): lax.all_to_all(copies, axis, split_axis=0, concat_axis=0, tiled=True)  8.03 us
    all_to_all x1, starting transfers between devices, side_by_side(): lax.all_to_all(copies, axis, split_axis=0, concat_axis=0, tiled=True)  7.32 us
  transfers between devices with their start and end apart: 27, of which 16 were waited for; matrix products, arithmetic and copies ran while one was open for 9% of the time, Pallas kernels for 0%

profile of v4, /device:TPU:80, one launch (start us, length us, event | category | flops | bytes accessed | tf_op | source)
XLA Modules:
  0.0 254.8 jit_solution(5127011117959189595)
XLA Ops:
  6.6 1.4 slice_bitcast_fusion.28
  8.0 1.6 pad_maximum_fusion.3
  9.7 0.7 slice.184
  10.4 1.8 collective-permute-start
  12.2 0.7 broadcast_in_dim.4
  12.9 7.3 %all-to-all-start = ((bf16[8,64,256]{2,1,0:T(8,128)(2,1)}), bf16[8,64,256]{2,1,0:T(8,128)(2,1)S(1)}, u32[]{:S(2)}, u32[]{:S(2)}) async-start(bf16[8,64,256]{2,1,0:T(8,128)(2,1)} %broadcast_in_dim.4), calls=%async_computation | async-start | bytes 524288 | tf_op jit(solution)/shard_map/all_to_all | solution.py:46
  20.4 1.0 constant_dynamic-update-slice_fusion
  21.4 3.9 %collective-permute-start.1 = (bf16[520,256]{1,0:T(8,128)(2,1)S(1)}, bf16[520,256]{1,0:T(8,128)(2,1)S(1)}, u32[]{:S(2)}, u32[]{:S(2)}) collective-permute-start(bf16[520,256]{1,0:T(8,128)(2,1)S(1)} %constant_dynamic-update-slice_fusion), channel_id=1, source_target_pairs={{0,1},{1,2},{2,3},{3,4},{4,5},{5,6},{6,7},{7,0},{8,9},{9,10},{10,1... | collective-permute-start | bytes 798728 | tf_op jit(solution)/shard_map/ppermute | solution.py:22
  25.2 3.3 %collective-permute-start.4 = (bf16[520,256]{1,0:T(8,128)(2,1)S(1)}, bf16[520,256]{1,0:T(8,128)(2,1)S(1)}, u32[]{:S(2)}, u32[]{:S(2)}) collective-permute-start(bf16[520,256]{1,0:T(8,128)(2,1)S(1)} %constant_dynamic-update-slice_fusion), channel_id=1, source_target_pairs={{0,7},{1,0},{2,1},{3,2},{4,3},{5,4},{6,5},{7,6},{8,15},{9,8},{10,9... | collective-permute-start | bytes 798728 | tf_op jit(solution)/shard_map/ppermute | solution.py:22
  28.5 0.8 slice_convert_fusion
  29.3 6.7 %collective-permute-done.1 = bf16[520,256]{1,0:T(8,128)(2,1)S(1)} collective-permute-done((bf16[520,256]{1,0:T(8,128)(2,1)S(1)}, bf16[520,256]{1,0:T(8,128)(2,1)S(1)}, u32[]{:S(2)}, u32[]{:S(2)}) %collective-permute-start.1) | collective-permute-done | bytes 266272 | tf_op jit(solution)/shard_map/ppermute | solution.py:22
  36.0 1.9 collective-permute-start.2
  37.9 5.2 %collective-permute-start.5 = (bf16[520,256]{1,0:T(8,128)(2,1)S(1)}, bf16[520,256]{1,0:T(8,128)(2,1)S(1)}, u32[]{:S(2)}, u32[]{:S(2)}) collective-permute-start(bf16[520,256]{1,0:T(8,128)(2,1)S(1)} %collective-permute-done.4), channel_id=1, source_target_pairs={{0,7},{1,0},{2,1},{3,2},{4,3},{5,4},{6,5},{7,6},{8,15},{9,8},{10,9... | collective-permute-start | bytes 798728 | tf_op jit(solution)/shard_map/ppermute | solution.py:22
  43.2 5.2 %collective-permute-done.2 = bf16[520,256]{1,0:T(8,128)(2,1)S(1)} collective-permute-done((bf16[520,256]{1,0:T(8,128)(2,1)S(1)}, bf16[520,256]{1,0:T(8,128)(2,1)S(1)}, u32[]{:S(2)}, u32[]{:S(2)}) %collective-permute-start.2) | collective-permute-done | bytes 266272 | tf_op jit(solution)/shard_map/ppermute | solution.py:22
  48.4 1.9 collective-permute-start.3
  50.3 5.2 %collective-permute-start.6 = (bf16[520,256]{1,0:T(8,128)(2,1)S(1)}, bf16[520,256]{1,0:T(8,128)(2,1)S(1)}, u32[]{:S(2)}, u32[]{:S(2)}) collective-permute-start(bf16[520,256]{1,0:T(8,128)(2,1)S(1)} %collective-permute-done.5), channel_id=1, source_target_pairs={{0,7},{1,0},{2,1},{3,2},{4,3},{5,4},{6,5},{7,6},{8,15},{9,8},{10,9... | collective-permute-start | bytes 798728 | tf_op jit(solution)/shard_map/ppermute | solution.py:22
  55.5 4.4 %collective-permute-done.3 = bf16[520,256]{1,0:T(8,128)(2,1)S(1)} collective-permute-done((bf16[520,256]{1,0:T(8,128)(2,1)S(1)}, bf16[520,256]{1,0:T(8,128)(2,1)S(1)}, u32[]{:S(2)}, u32[]{:S(2)}) %collective-permute-start.3) | collective-permute-done | bytes 266272 | tf_op jit(solution)/shard_map/ppermute | solution.py:22
  60.0 3.5 %collective-permute-start.7 = (bf16[520,256]{1,0:T(8,128)(2,1)S(1)}, bf16[520,256]{1,0:T(8,128)(2,1)S(1)}, u32[]{:S(2)}, u32[]{:S(2)}) collective-permute-start(bf16[520,256]{1,0:T(8,128)(2,1)S(1)} %constant_dynamic-update-slice_fusion), channel_id=1, source_target_pairs={{0,4},{1,5},{2,6},{3,7},{4,0},{5,1},{6,2},{7,3},{8,12},{9,13},{10,... | collective-permute-start | bytes 798728 | tf_op jit(solution)/shard_map/ppermute | solution.py:22
  63.6 15.0 %collective-permute-done.7 = bf16[520,256]{1,0:T(8,128)(2,1)S(1)} collective-permute-done((bf16[520,256]{1,0:T(8,128)(2,1)S(1)}, bf16[520,256]{1,0:T(8,128)(2,1)S(1)}, u32[]{:S(2)}, u32[]{:S(2)}) %collective-permute-start.7) | collective-permute-done | bytes 266272 | tf_op jit(solution)/shard_map/ppermute | solution.py:22
  79.0 0.5 fusion
  79.5 2.7 %fusion.3 = (bf16[520,2048]{1,0:T(8,128)(2,1)}, bf16[520,2048]{1,0:T(8,128)(2,1)}) fusion(f32[2048]{0:T(1024)S(1)} %bitcast.133, bf16[520,4096]{1,0:T(8,128)(2,1)S(1)} %constant_dynamic-update-slice_fusion.10, s32[]{:T(128)S(6)} %select_n.118, f32[2048]{0:T(1024)S(1)} %bitcast.135, f32[520]{0:T(1024)S(1)} %add_rsqrt_fusion.1), kind=kLoop, calls=%fused_computation.6 | loop fusion | flops 6389760 | bytes 6408228 | tf_op jit(solution)/shard_map/convert_element_type | solution.py:152
  82.2 0.7 multiply_convert_fusion.4.rows
  83.0 39.3 %all-gather.3.cloned.1.call-done.weight = bf16[7,2048,256]{2,1,0:T(8,128)(2,1)} async-done(((bf16[7,64,256]{2,1,0:T(8,128)(2,1)}), bf16[7,2048,256]{2,1,0:T(8,128)(2,1)}) %all-gather.3.cloned.1.call-update) | async-done | bytes 7340048 | tf_op jit(solution)/shard_map/all_gather | solution.py:145
  122.3 3.9 %shard_map.73 = bf16[4,64,256]{2,1,0:T(8,128)(2,1)} custom-call(bf16[64,2048]{1,0:T(8,128)(2,1)} %multiply_convert_fusion.4.rows, bf16[7,2048,256]{2,1,0:T(8,128)(2,1)} %all-gather.3.cloned.1.call-done.weight, bf16[64,256]{1,0:T(8,128)(2,1)} %get-tuple-element.33.own), custom_call_target="tpu_custom_call" | custom-call | flops 201326592 | bytes 3145728 | tf_op jit(solution)/shard_map/pallas_call | solution.py:103
  126.3 2.7 %fusion.9 = f32[520,256]{1,0:T(8,128)S(1)} fusion(bf16[520,2048]{1,0:T(8,128)(2,1)} %get-tuple-element.18, bf16[7,2048,256]{2,1,0:T(8,128)(2,1)} %all-gather.3.cloned.1.call-done.weight), kind=kOutput, calls=%fused_computation.15 | convolution fusion | flops 545525760 | bytes 3710976 | tf_op jit(solution)/shard_map/dot_general | solution.py:87
  129.1 2.1 fusion.8
  131.2 0.8 fusion.6
  132.0 3.7 %collective-permute-start.8 = (bf16[520,256]{1,0:T(8,128)(2,1)S(1)}, bf16[520,256]{1,0:T(8,128)(2,1)S(1)}, u32[]{:S(2)}, u32[]{:S(2)}) collective-permute-start(bf16[520,256]{1,0:T(8,128)(2,1)S(1)} %fusion.6), channel_id=1, source_target_pairs={{0,1},{1,2},{2,3},{3,4},{4,5},{5,6},{6,7},{7,0},{8,9},{9,10},{10,1... | collective-permute-start | bytes 798728 | tf_op jit(solution)/shard_map/ppermute | solution.py:22
  135.7 3.4 %collective-permute-start.11 = (bf16[520,256]{1,0:T(8,128)(2,1)S(1)}, bf16[520,256]{1,0:T(8,128)(2,1)S(1)}, u32[]{:S(2)}, u32[]{:S(2)}) collective-permute-start(bf16[520,256]{1,0:T(8,128)(2,1)S(1)} %fusion.6), channel_id=1, source_target_pairs={{0,7},{1,0},{2,1},{3,2},{4,3},{5,4},{6,5},{7,6},{8,15},{9,8},{10,9... | collective-permute-start | bytes 798728 | tf_op jit(solution)/shard_map/ppermute | solution.py:22
  139.1 1.6 fusion.24
  140.7 3.1 %collective-permute-done.8 = bf16[520,256]{1,0:T(8,128)(2,1)S(1)} collective-permute-done((bf16[520,256]{1,0:T(8,128)(2,1)S(1)}, bf16[520,256]{1,0:T(8,128)(2,1)S(1)}, u32[]{:S(2)}, u32[]{:S(2)}) %collective-permute-start.8) | collective-permute-done | bytes 266272 | tf_op jit(solution)/shard_map/ppermute | solution.py:22
  143.8 2.4 collective-permute-start.9
  146.1 1.6 fusion.25
  147.7 4.7 %collective-permute-start.12 = (bf16[520,256]{1,0:T(8,128)(2,1)S(1)}, bf16[520,256]{1,0:T(8,128)(2,1)S(1)}, u32[]{:S(2)}, u32[]{:S(2)}) collective-permute-start(bf16[520,256]{1,0:T(8,128)(2,1)S(1)} %collective-permute-done.11), channel_id=1, source_target_pairs={{0,7},{1,0},{2,1},{3,2},{4,3},{5,4},{6,5},{7,6},{8,15},{9,8},{10,9... | collective-permute-start | bytes 798728 | tf_op jit(solution)/shard_map/ppermute | solution.py:22
  152.4 2.2 collective-permute-done.9
  154.7 1.9 collective-permute-start.10
  156.6 1.6 fusion.26
  158.2 5.2 %collective-permute-start.13 = (bf16[520,256]{1,0:T(8,128)(2,1)S(1)}, bf16[520,256]{1,0:T(8,128)(2,1)S(1)}, u32[]{:S(2)}, u32[]{:S(2)}) collective-permute-start(bf16[520,256]{1,0:T(8,128)(2,1)S(1)} %collective-permute-done.12), channel_id=1, source_target_pairs={{0,7},{1,0},{2,1},{3,2},{4,3},{5,4},{6,5},{7,6},{8,15},{9,8},{10,9... | collective-permute-start | bytes 798728 | tf_op jit(solution)/shard_map/ppermute | solution.py:22
  163.4 1.4 collective-permute-done.10
  164.9 7.3 %collective-permute-start.14 = (bf16[520,256]{1,0:T(8,128)(2,1)S(1)}, bf16[520,256]{1,0:T(8,128)(2,1)S(1)}, u32[]{:S(2)}, u32[]{:S(2)}) collective-permute-start(bf16[520,256]{1,0:T(8,128)(2,1)S(1)} %fusion.6), channel_id=1, source_target_pairs={{0,4},{1,5},{2,6},{3,7},{4,0},{5,1},{6,2},{7,3},{8,12},{9,13},{10,... | collective-permute-start | bytes 798728 | tf_op jit(solution)/shard_map/ppermute | solution.py:22
  172.3 10.2 %collective-permute-done.14 = bf16[520,256]{1,0:T(8,128)(2,1)S(1)} collective-permute-done((bf16[520,256]{1,0:T(8,128)(2,1)S(1)}, bf16[520,256]{1,0:T(8,128)(2,1)S(1)}, u32[]{:S(2)}, u32[]{:S(2)}) %collective-permute-start.14) | collective-permute-done | bytes 266272 | tf_op jit(solution)/shard_map/ppermute | solution.py:22
  183.0 0.5 copy-done.11
  183.5 0.9 multiply_reduce_fusion
  184.9 0.6 broadcast_in_dim.5
  185.5 4.2 %all-to-all-start.1 = ((f32[8,5,128]{2,1,0:T(8,128)}), f32[8,5,128]{2,1,0:T(8,128)S(1)}, u32[]{:S(2)}, u32[]{:S(2)}) async-start(f32[8,5,128]{2,1,0:T(8,128)} %broadcast_in_dim.5), calls=%async_computation.1 | async-start | bytes 65536 | tf_op jit(solution)/shard_map/all_to_all | solution.py:54
  189.7 8.0 %all-to-all-done.1 = f32[8,5,128]{2,1,0:T(8,128)S(1)} async-done(((f32[8,5,128]{2,1,0:T(8,128)}), f32[8,5,128]{2,1,0:T(8,128)S(1)}, u32[]{:S(2)}, u32[]{:S(2)}) %all-to-all-start.1) | async-done | bytes 20512 | tf_op jit(solution)/shard_map/all_to_all | solution.py:54
  197.8 0.7 all-gather.5.cloned.1.call-done
  198.5 2.7 %fusion.20 = f32[520,256]{1,0:T(8,128)S(1)} fusion(bf16[520,2048]{1,0:T(8,128)(2,1)} %copy-done.1, bf16[4,2048,256]{2,1,0:T(8,128)(2,1)} %all-gather.5.cloned.1.call-done), kind=kOutput, calls=%fused_computation.35 | convolution fusion | flops 545259520 | bytes 3710976 | tf_op jit(solution)/shard_map/dot_general | solution.py:87
  201.6 0.8 fusion.21
  203.1 0.8 fusion.22
  204.1 3.5 %collective-permute-start.15 = (bf16[256,256]{1,0:T(8,128)(2,1)S(1)}, bf16[256,256]{1,0:T(8,128)(2,1)S(1)}, u32[]{:S(2)}, u32[]{:S(2)}) collective-permute-start(bf16[256,256]{1,0:T(8,128)(2,1)S(1)} %get-tuple-element.31), channel_id=1, source_target_pairs={{0,1},{1,0},{2,3},{3,2},{4,5},{5,4},{6,7},{7,6},{8,15},{9,10},{10,... | collective-permute-start | bytes 393224 | tf_op jit(solution)/shard_map/ppermute | solution.py:64
  207.6 2.4 collective-permute-start.19
  210.3 0.7 collective-permute-done.15
  211.1 4.8 %collective-permute-start.16 = (bf16[512,256]{1,0:T(8,128)(2,1)S(1)}, bf16[512,256]{1,0:T(8,128)(2,1)S(1)}, u32[]{:S(2)}, u32[]{:S(2)}) collective-permute-start(bf16[512,256]{1,0:T(8,128)(2,1)S(1)} %pad_maximum_fusion), channel_id=1, source_target_pairs={{0,7},{1,2},{2,1},{3,4},{4,3},{5,6},{6,5},{7,0},{8,9},{9,8},{10,11... | collective-permute-start | bytes 786440 | tf_op jit(solution)/shard_map/ppermute | solution.py:64
  215.9 3.2 %collective-permute-start.20 = (bf16[512,256]{1,0:T(8,128)(2,1)S(1)}, bf16[512,256]{1,0:T(8,128)(2,1)S(1)}, u32[]{:S(2)}, u32[]{:S(2)}) collective-permute-start(bf16[512,256]{1,0:T(8,128)(2,1)S(1)} %pad_maximum_fusion.1), channel_id=1, source_target_pairs={{0,7},{1,2},{2,1},{3,4},{4,3},{5,6},{6,5},{7,0},{8,9},{9,8},{10,11... | collective-permute-start | bytes 786440 | tf_op jit(solution)/shard_map/ppermute | solution.py:64
  219.4 1.2 collective-permute-done.16
  220.6 2.3 collective-permute-start.17
  223.0 3.3 %collective-permute-done.20 = bf16[512,256]{1,0:T(8,128)(2,1)S(1)} collective-permute-done((bf16[512,256]{1,0:T(8,128)(2,1)S(1)}, bf16[512,256]{1,0:T(8,128)(2,1)S(1)}, u32[]{:S(2)}, u32[]{:S(2)}) %collective-permute-start.20) | collective-permute-done | bytes 262176 | tf_op jit(solution)/shard_map/ppermute | solution.py:64
  226.5 2.0 collective-permute-start.21
  229.3 4.3 %collective-permute-start.18 = (bf16[512,256]{1,0:T(8,128)(2,1)S(1)}, bf16[512,256]{1,0:T(8,128)(2,1)S(1)}, u32[]{:S(2)}, u32[]{:S(2)}) collective-permute-start(bf16[512,256]{1,0:T(8,128)(2,1)S(1)} %collective-permute-done.17), channel_id=1, source_target_pairs={{0,7},{1,2},{2,1},{3,4},{4,3},{5,6},{6,5},{7,0},{8,9},{9,8},{10,11... | collective-permute-start | bytes 786440 | tf_op jit(solution)/shard_map/ppermute | solution.py:64
  233.9 3.2 %collective-permute-done.21 = bf16[512,256]{1,0:T(8,128)(2,1)S(1)} collective-permute-done((bf16[512,256]{1,0:T(8,128)(2,1)S(1)}, bf16[512,256]{1,0:T(8,128)(2,1)S(1)}, u32[]{:S(2)}, u32[]{:S(2)}) %collective-permute-start.21) | collective-permute-done | bytes 262176 | tf_op jit(solution)/shard_map/ppermute | solution.py:64
  237.1 1.9 collective-permute-start.22
  239.9 6.7 %collective-permute-done.22 = bf16[512,256]{1,0:T(8,128)(2,1)S(1)} collective-permute-done((bf16[512,256]{1,0:T(8,128)(2,1)S(1)}, bf16[512,256]{1,0:T(8,128)(2,1)S(1)}, u32[]{:S(2)}, u32[]{:S(2)}) %collective-permute-start.22) | collective-permute-done | bytes 262176 | tf_op jit(solution)/shard_map/ppermute | solution.py:64
  247.2 0.7 pad_maximum_fusion.2
  (114 shorter events, 6.3 us)
Async XLA Ops:
  6.5 53.4 %copy-start = (bf16[512,256]{1,0:T(8,128)(2,1)S(1)}, bf16[512,256]{1,0:T(8,128)(2,1)}, u32[]{:S(2)}) copy-start(bf16[512,256]{1,0:T(8,128)(2,1)} %param.7) | copy-start | bytes 786436
  6.5 115.7 %all-gather.3.cloned.1.call-start = ((), (), s32[]{:S(2)}) async-start(), calls=%async_computation.2 | async-start | bytes 7569408 | tf_op jit(solution)/shard_map/all_gather | solution.py:145
  10.4 10.0 %collective-permute-start = (bf16[8,256]{1,0:T(8,128)(2,1)S(1)}, bf16[8,256]{1,0:T(8,128)(2,1)S(1)}, u32[]{:S(2)}, u32[]{:S(2)}) collective-permute-start(bf16[8,256]{1,0:T(8,128)(2,1)S(1)} %slice.184), channel_id=1, source_target_pairs={{0,8},{8,16},{16,24},{24,32},{32,40},{40,48},{48,56},{56,64},{64,7... | collective-permute-start | bytes 12296 | tf_op jit(solution)/shard_map/ppermute | solution.py:17
  12.9 30.2 %all-to-all-start = ((bf16[8,64,256]{2,1,0:T(8,128)(2,1)}), bf16[8,64,256]{2,1,0:T(8,128)(2,1)S(1)}, u32[]{:S(2)}, u32[]{:S(2)}) async-start(bf16[8,64,256]{2,1,0:T(8,128)(2,1)} %broadcast_in_dim.4), calls=%async_computation | async-start | bytes 524288 | tf_op jit(solution)/shard_map/all_to_all | solution.py:46
  20.3 178.2 %all-gather.5.cloned.1.call-start = ((), (), s32[]{:S(2)}) async-start(), calls=%async_computation.3 | async-start | bytes 4325376 | tf_op jit(solution)/shard_map/all_gather | solution.py:157
  21.3 57.6 %copy-start.10 = (bf16[520,256]{1,0:T(8,128)(2,1)}, bf16[520,256]{1,0:T(8,128)(2,1)S(1)}, u32[]{:S(2)}) copy-start(bf16[520,256]{1,0:T(8,128)(2,1)S(1)} %constant_dynamic-update-slice_fusion) | copy-start | bytes 798724
  21.4 14.6 %collective-permute-start.1 = (bf16[520,256]{1,0:T(8,128)(2,1)S(1)}, bf16[520,256]{1,0:T(8,128)(2,1)S(1)}, u32[]{:S(2)}, u32[]{:S(2)}) collective-permute-start(bf16[520,256]{1,0:T(8,128)(2,1)S(1)} %constant_dynamic-update-slice_fusion), channel_id=1, source_target_pairs={{0,1},{1,2},{2,3},{3,4},{4,5},{5,6},{6,7},{7,0},{8,9},{9,10},{10,1... | collective-permute-start | bytes 798728 | tf_op jit(solution)/shard_map/ppermute | solution.py:22
  25.2 12.7 %collective-permute-start.4 = (bf16[520,256]{1,0:T(8,128)(2,1)S(1)}, bf16[520,256]{1,0:T(8,128)(2,1)S(1)}, u32[]{:S(2)}, u32[]{:S(2)}) collective-permute-start(bf16[520,256]{1,0:T(8,128)(2,1)S(1)} %constant_dynamic-update-slice_fusion), channel_id=1, source_target_pairs={{0,7},{1,0},{2,1},{3,2},{4,3},{5,4},{6,5},{7,6},{8,15},{9,8},{10,9... | collective-permute-start | bytes 798728 | tf_op jit(solution)/shard_map/ppermute | solution.py:22
  36.0 12.4 %collective-permute-start.2 = (bf16[520,256]{1,0:T(8,128)(2,1)S(1)}, bf16[520,256]{1,0:T(8,128)(2,1)S(1)}, u32[]{:S(2)}, u32[]{:S(2)}) collective-permute-start(bf16[520,256]{1,0:T(8,128)(2,1)S(1)} %collective-permute-done.1), channel_id=1, source_target_pairs={{0,1},{1,2},{2,3},{3,4},{4,5},{5,6},{6,7},{7,0},{8,9},{9,10},{10,1... | collective-permute-start | bytes 798728 | tf_op jit(solution)/shard_map/ppermute | solution.py:22
  37.9 12.4 %collective-permute-start.5 = (bf16[520,256]{1,0:T(8,128)(2,1)S(1)}, bf16[520,256]{1,0:T(8,128)(2,1)S(1)}, u32[]{:S(2)}, u32[]{:S(2)}) collective-permute-start(bf16[520,256]{1,0:T(8,128)(2,1)S(1)} %collective-permute-done.4), channel_id=1, source_target_pairs={{0,7},{1,0},{2,1},{3,2},{4,3},{5,4},{6,5},{7,6},{8,15},{9,8},{10,9... | collective-permute-start | bytes 798728 | tf_op jit(solution)/shard_map/ppermute | solution.py:22
  48.4 11.5 %collective-permute-start.3 = (bf16[520,256]{1,0:T(8,128)(2,1)S(1)}, bf16[520,256]{1,0:T(8,128)(2,1)S(1)}, u32[]{:S(2)}, u32[]{:S(2)}) collective-permute-start(bf16[520,256]{1,0:T(8,128)(2,1)S(1)} %collective-permute-done.2), channel_id=1, source_target_pairs={{0,1},{1,2},{2,3},{3,4},{4,5},{5,6},{6,7},{7,0},{8,9},{9,10},{10,1... | collective-permute-start | bytes 798728 | tf_op jit(solution)/shard_map/ppermute | solution.py:22
  50.3 13.3 %collective-permute-start.6 = (bf16[520,256]{1,0:T(8,128)(2,1)S(1)}, bf16[520,256]{1,0:T(8,128)(2,1)S(1)}, u32[]{:S(2)}, u32[]{:S(2)}) collective-permute-start(bf16[520,256]{1,0:T(8,128)(2,1)S(1)} %collective-permute-done.5), channel_id=1, source_target_pairs={{0,7},{1,0},{2,1},{3,2},{4,3},{5,4},{6,5},{7,6},{8,15},{9,8},{10,9... | collective-permute-start | bytes 798728 | tf_op jit(solution)/shard_map/ppermute | solution.py:22
  60.0 18.6 %collective-permute-start.7 = (bf16[520,256]{1,0:T(8,128)(2,1)S(1)}, bf16[520,256]{1,0:T(8,128)(2,1)S(1)}, u32[]{:S(2)}, u32[]{:S(2)}) collective-permute-start(bf16[520,256]{1,0:T(8,128)(2,1)S(1)} %constant_dynamic-update-slice_fusion), channel_id=1, source_target_pairs={{0,4},{1,5},{2,6},{3,7},{4,0},{5,1},{6,2},{7,3},{8,12},{9,13},{10,... | collective-permute-start | bytes 798728 | tf_op jit(solution)/shard_map/ppermute | solution.py:22
  82.2 44.1 %copy-start.9 = (bf16[2,3,256]{2,0,1:T(2,128)(2,1)S(1)}, bf16[2,3,256]{2,0,1:T(2,128)(2,1)}, u32[]{:S(2)}) copy-start(bf16[2,3,256]{2,0,1:T(2,128)(2,1)} %param.13) | copy-start | bytes 9220
  122.3 8.9 %slice-start = ((s8[7340032]{0:T(1024)(128)(4,1)}), s8[3145728]{0:T(1024)(128)(4,1)S(1)}, s32[]{:S(2)}) async-start(s8[7340032]{0:T(1024)(128)(4,1)} %bitcast.131), calls=%async_computation.4 | async-start | bytes 6291456
  126.3 2.8 %copy-start.4 = (bf16[520,2048]{1,0:T(8,128)(2,1)S(1)}, bf16[520,2048]{1,0:T(8,128)(2,1)}, u32[]{:S(2)}) copy-start(bf16[520,2048]{1,0:T(8,128)(2,1)} %get-tuple-element.18) | copy-start | bytes 6389764
  126.3 4.8 %slice-start.1 = ((s8[7340032]{0:T(1024)(128)(4,1)}), s8[4194304]{0:T(1024)(128)(4,1)S(1)}, s32[]{:S(2)}) async-start(s8[7340032]{0:T(1024)(128)(4,1)} %bitcast.131), calls=%async_computation.5 | async-start | bytes 8388608
  131.2 7.9 %copy-start.3 = (bf16[520,2048]{1,0:T(8,128)(2,1)S(1)}, bf16[520,2048]{1,0:T(8,128)(2,1)}, u32[]{:S(2)}) copy-start(bf16[520,2048]{1,0:T(8,128)(2,1)} %get-tuple-element.21) | copy-start | bytes 6389764
  132.0 11.8 %collective-permute-start.8 = (bf16[520,256]{1,0:T(8,128)(2,1)S(1)}, bf16[520,256]{1,0:T(8,128)(2,1)S(1)}, u32[]{:S(2)}, u32[]{:S(2)}) collective-permute-start(bf16[520,256]{1,0:T(8,128)(2,1)S(1)} %fusion.6), channel_id=1, source_target_pairs={{0,1},{1,2},{2,3},{3,4},{4,5},{5,6},{6,7},{7,0},{8,9},{9,10},{10,1... | collective-permute-start | bytes 798728 | tf_op jit(solution)/shard_map/ppermute | solution.py:22
  135.7 12.0 %collective-permute-start.11 = (bf16[520,256]{1,0:T(8,128)(2,1)S(1)}, bf16[520,256]{1,0:T(8,128)(2,1)S(1)}, u32[]{:S(2)}, u32[]{:S(2)}) collective-permute-start(bf16[520,256]{1,0:T(8,128)(2,1)S(1)} %fusion.6), channel_id=1, source_target_pairs={{0,7},{1,0},{2,1},{3,2},{4,3},{5,4},{6,5},{7,6},{8,15},{9,8},{10,9... | collective-permute-start | bytes 798728 | tf_op jit(solution)/shard_map/ppermute | solution.py:22
  143.8 10.9 %collective-permute-start.9 = (bf16[520,256]{1,0:T(8,128)(2,1)S(1)}, bf16[520,256]{1,0:T(8,128)(2,1)S(1)}, u32[]{:S(2)}, u32[]{:S(2)}) collective-permute-start(bf16[520,256]{1,0:T(8,128)(2,1)S(1)} %collective-permute-done.8), channel_id=1, source_target_pairs={{0,1},{1,2},{2,3},{3,4},{4,5},{5,6},{6,7},{7,0},{8,9},{9,10},{10,1... | collective-permute-start | bytes 798728 | tf_op jit(solution)/shard_map/ppermute | solution.py:22
  147.7 10.5 %collective-permute-start.12 = (bf16[520,256]{1,0:T(8,128)(2,1)S(1)}, bf16[520,256]{1,0:T(8,128)(2,1)S(1)}, u32[]{:S(2)}, u32[]{:S(2)}) collective-permute-start(bf16[520,256]{1,0:T(8,128)(2,1)S(1)} %collective-permute-done.11), channel_id=1, source_target_pairs={{0,7},{1,0},{2,1},{3,2},{4,3},{5,4},{6,5},{7,6},{8,15},{9,8},{10,9... | collective-permute-start | bytes 798728 | tf_op jit(solution)/shard_map/ppermute | solution.py:22
  154.7 10.1 %collective-permute-start.10 = (bf16[520,256]{1,0:T(8,128)(2,1)S(1)}, bf16[520,256]{1,0:T(8,128)(2,1)S(1)}, u32[]{:S(2)}, u32[]{:S(2)}) collective-permute-start(bf16[520,256]{1,0:T(8,128)(2,1)S(1)} %collective-permute-done.9), channel_id=1, source_target_pairs={{0,1},{1,2},{2,3},{3,4},{4,5},{5,6},{6,7},{7,0},{8,9},{9,10},{10,1... | collective-permute-start | bytes 798728 | tf_op jit(solution)/shard_map/ppermute | solution.py:22
  158.2 14.1 %collective-permute-start.13 = (bf16[520,256]{1,0:T(8,128)(2,1)S(1)}, bf16[520,256]{1,0:T(8,128)(2,1)S(1)}, u32[]{:S(2)}, u32[]{:S(2)}) collective-permute-start(bf16[520,256]{1,0:T(8,128)(2,1)S(1)} %collective-permute-done.12), channel_id=1, source_target_pairs={{0,7},{1,0},{2,1},{3,2},{4,3},{5,4},{6,5},{7,6},{8,15},{9,8},{10,9... | collective-permute-start | bytes 798728 | tf_op jit(solution)/shard_map/ppermute | solution.py:22
  164.9 17.6 %collective-permute-start.14 = (bf16[520,256]{1,0:T(8,128)(2,1)S(1)}, bf16[520,256]{1,0:T(8,128)(2,1)S(1)}, u32[]{:S(2)}, u32[]{:S(2)}) collective-permute-start(bf16[520,256]{1,0:T(8,128)(2,1)S(1)} %fusion.6), channel_id=1, source_target_pairs={{0,4},{1,5},{2,6},{3,7},{4,0},{5,1},{6,2},{7,3},{8,12},{9,13},{10,... | collective-permute-start | bytes 798728 | tf_op jit(solution)/shard_map/ppermute | solution.py:22
  182.5 1.0 copy-start.11
  183.5 1.3 copy-start.1
  184.9 16.4 %copy-start.2 = (bf16[520,2048]{1,0:T(8,128)(2,1)S(1)}, bf16[520,2048]{1,0:T(8,128)(2,1)}, u32[]{:S(2)}) copy-start(bf16[520,2048]{1,0:T(8,128)(2,1)} %copy-done.1) | copy-start | bytes 6389764
  185.5 12.3 %all-to-all-start.1 = ((f32[8,5,128]{2,1,0:T(8,128)}), f32[8,5,128]{2,1,0:T(8,128)S(1)}, u32[]{:S(2)}, u32[]{:S(2)}) async-start(f32[8,5,128]{2,1,0:T(8,128)} %broadcast_in_dim.5), calls=%async_computation.1 | async-start | bytes 65536 | tf_op jit(solution)/shard_map/all_to_all | solution.py:54
  198.5 3.1 %copy-start.8 = (bf16[4,2048,256]{2,1,0:T(8,128)(2,1)S(1)}, bf16[4,2048,256]{2,1,0:T(8,128)(2,1)}, u32[]{:S(2)}) copy-start(bf16[4,2048,256]{2,1,0:T(8,128)(2,1)} %all-gather.5.cloned.1.call-done) | copy-start | bytes 12582916
  201.6 1.0 copy-start.5
  201.6 1.2 copy-start.6
  202.8 1.0 copy-start.7
  204.1 6.9 %collective-permute-start.15 = (bf16[256,256]{1,0:T(8,128)(2,1)S(1)}, bf16[256,256]{1,0:T(8,128)(2,1)S(1)}, u32[]{:S(2)}, u32[]{:S(2)}) collective-permute-start(bf16[256,256]{1,0:T(8,128)(2,1)S(1)} %get-tuple-element.31), channel_id=1, source_target_pairs={{0,1},{1,0},{2,3},{3,2},{4,5},{5,4},{6,7},{7,6},{8,15},{9,10},{10,... | collective-permute-start | bytes 393224 | tf_op jit(solution)/shard_map/ppermute | solution.py:64
  207.6 8.2 %collective-permute-start.19 = (bf16[256,256]{1,0:T(8,128)(2,1)S(1)}, bf16[256,256]{1,0:T(8,128)(2,1)S(1)}, u32[]{:S(2)}, u32[]{:S(2)}) collective-permute-start(bf16[256,256]{1,0:T(8,128)(2,1)S(1)} %get-tuple-element.32), channel_id=1, source_target_pairs={{0,1},{1,0},{2,3},{3,2},{4,5},{5,4},{6,7},{7,6},{8,15},{9,10},{10,... | collective-permute-start | bytes 393224 | tf_op jit(solution)/shard_map/ppermute | solution.py:64
  211.1 9.5 %collective-permute-start.16 = (bf16[512,256]{1,0:T(8,128)(2,1)S(1)}, bf16[512,256]{1,0:T(8,128)(2,1)S(1)}, u32[]{:S(2)}, u32[]{:S(2)}) collective-permute-start(bf16[512,256]{1,0:T(8,128)(2,1)S(1)} %pad_maximum_fusion), channel_id=1, source_target_pairs={{0,7},{1,2},{2,1},{3,4},{4,3},{5,6},{6,5},{7,0},{8,9},{9,8},{10,11... | collective-permute-start | bytes 786440 | tf_op jit(solution)/shard_map/ppermute | solution.py:64
  215.9 10.4 %collective-permute-start.20 = (bf16[512,256]{1,0:T(8,128)(2,1)S(1)}, bf16[512,256]{1,0:T(8,128)(2,1)S(1)}, u32[]{:S(2)}, u32[]{:S(2)}) collective-permute-start(bf16[512,256]{1,0:T(8,128)(2,1)S(1)} %pad_maximum_fusion.1), channel_id=1, source_target_pairs={{0,7},{1,2},{2,1},{3,4},{4,3},{5,6},{6,5},{7,0},{8,9},{9,8},{10,11... | collective-permute-start | bytes 786440 | tf_op jit(solution)/shard_map/ppermute | solution.py:64
  220.6 8.7 %collective-permute-start.17 = (bf16[512,256]{1,0:T(8,128)(2,1)S(1)}, bf16[512,256]{1,0:T(8,128)(2,1)S(1)}, u32[]{:S(2)}, u32[]{:S(2)}) collective-permute-start(bf16[512,256]{1,0:T(8,128)(2,1)S(1)} %collective-permute-done.16), channel_id=1, source_target_pairs={{0,1},{1,0},{2,3},{3,2},{4,5},{5,4},{6,7},{7,6},{8,15},{9,10},{10,... | collective-permute-start | bytes 786440 | tf_op jit(solution)/shard_map/ppermute | solution.py:64
  226.5 10.6 %collective-permute-start.21 = (bf16[512,256]{1,0:T(8,128)(2,1)S(1)}, bf16[512,256]{1,0:T(8,128)(2,1)S(1)}, u32[]{:S(2)}, u32[]{:S(2)}) collective-permute-start(bf16[512,256]{1,0:T(8,128)(2,1)S(1)} %collective-permute-done.20), channel_id=1, source_target_pairs={{0,1},{1,0},{2,3},{3,2},{4,5},{5,4},{6,7},{7,6},{8,15},{9,10},{10,... | collective-permute-start | bytes 786440 | tf_op jit(solution)/shard_map/ppermute | solution.py:64
  229.3 10.3 %collective-permute-start.18 = (bf16[512,256]{1,0:T(8,128)(2,1)S(1)}, bf16[512,256]{1,0:T(8,128)(2,1)S(1)}, u32[]{:S(2)}, u32[]{:S(2)}) collective-permute-start(bf16[512,256]{1,0:T(8,128)(2,1)S(1)} %collective-permute-done.17), channel_id=1, source_target_pairs={{0,7},{1,2},{2,1},{3,4},{4,3},{5,6},{6,5},{7,0},{8,9},{9,8},{10,11... | collective-permute-start | bytes 786440 | tf_op jit(solution)/shard_map/ppermute | solution.py:64
  237.1 9.5 %collective-permute-start.22 = (bf16[512,256]{1,0:T(8,128)(2,1)S(1)}, bf16[512,256]{1,0:T(8,128)(2,1)S(1)}, u32[]{:S(2)}, u32[]{:S(2)}) collective-permute-start(bf16[512,256]{1,0:T(8,128)(2,1)S(1)} %collective-permute-done.21), channel_id=1, source_target_pairs={{0,7},{1,2},{2,1},{3,4},{4,3},{5,6},{6,5},{7,0},{8,9},{9,8},{10,11... | collective-permute-start | bytes 786440 | tf_op jit(solution)/shard_map/ppermute | solution.py:64
Sparse Core Ops, SparseCore 0:
  9.8 112.4 all-gather.2
  126.4 72.0 all-gather.4
